TPU v7x, 128 devices: a whole 4x4x4 slice. The times are simulated.
128 devices in a mesh: sp: 8 (over x, core), tp: 16 (over z, y).
Axes of the slice: x: 4, y: 4, z: 4, core: 2. Of those that a mesh axis runs over, the one named last changes fastest.
Arguments:
- tokens: bfloat16 [4, 2048, 2048], P(None, ('sp', 'tp')), may hold values from -6 to 6
- norm_gain: float32 [2048], replicated, may hold values from 0.5 to 1.5
- entry_projection: bfloat16 [2048, 2048], P(None, 'tp'), may hold values from -0.125 to 0.125
- valve_projection: bfloat16 [2048, 2048], P(None, 'tp'), may hold values from -0.125 to 0.125
- filter_taps: float32 [4, 2048], P(None, 'tp'), may hold values from -3 to 3
- conv_bias: float32 [2048], P('tp'), may hold values from -0.6 to 0.6
- recur_weight: bfloat16 [16, 128, 128], P('tp'), may hold values from -0.5 to 0.5
- recur_bias: float32 [2048], P('tp'), may hold values from -3 to 3
- entry_weight: bfloat16 [16, 128, 128], P('tp'), may hold values from -0.5 to 0.5
- entry_bias: float32 [2048], P('tp'), may hold values from -0.6 to 0.6
- forget_rate: float32 [2048], P('tp'), may hold values from 3.0517578e-05 to 0.25, as said below
- output_weight: bfloat16 [2048, 2048], P('tp'), may hold values from -0.5 to 0.5
Outputs:
- mixed: bfloat16 [4, 2048, 2048], P(None, ('sp', 'tp'))
Inputs may be any that keep to these rules, and one draw needn't show every extreme that they name: forget_rate is positive; its even channels lie between 1 / 32768 and 1 / 8192, its odd channels between 1 / 64 and 1 / 4.
All inputs are finite; a program needn't handle non-finite values.
Results may differ from a plain program's by a relative error of at most 0.02.
Values may be sent and summed in bfloat16 or wider, within the bound.
No kernel may reach another device: no remote copies, remote signals or barrier semaphores. Data moves between devices by JAX's collectives and lax.ppermute only.
A program may use at most 64 MiB of HBM per device.

v0:
```python
import functools

import jax
import jax.numpy as jnp
from jax import lax
from jax.experimental import pallas as pl
from jax.experimental.pallas import tpu as pltpu
from jax.sharding import Mesh
from jax.sharding import PartitionSpec as P


TP = ("z", "y")
SP_TP = ("x", "c", "z", "y")
EPS = 1e-06
GATE_POWER = 8.0
F32 = jnp.float32
BF16 = jnp.bfloat16
HALF = 1024
SHIFTS = (1, -1, 2)
SOURCES = (0, 3, 1, 2)


def shift(value, axis, by):
    size = lax.axis_size(axis)
    return lax.ppermute(value, axis, [(i, (i + by) % size) for i in range(size)])


def spread(value, axis):
    return [shift(value, axis, by) for by in SHIFTS]


def swap_cores(values):
    return [shift(v, "c", 1) for v in values]


def call(kernel, idx, ins, outs, scratch=(), far=0, to_hbm=False):
    vmem = pl.BlockSpec(memory_space=pltpu.VMEM)
    anywhere = pl.BlockSpec(memory_space=pltpu.HBM)
    hold = jax.ShapeDtypeStruct if to_hbm else pltpu.VMEM
    return pl.pallas_call(
        kernel,
        out_shape=[hold(s, d) for s, d in outs],
        in_specs=[pl.BlockSpec(memory_space=pltpu.SMEM)]
        + [anywhere if k < far else vmem for k in range(len(ins))],
        out_specs=[vmem] * len(outs),
        scratch_shapes=list(scratch),
        compiler_params=pltpu.CompilerParams(vmem_limit_bytes=16 << 20),
    )(
        idx,
        *[
            pltpu.with_memory_space_constraint(a, pltpu.HBM if k < far else pltpu.VMEM)
            for k, a in enumerate(ins)
        ],
    )


def fetch_kernel(
    idx, entry, valve, ow, tokens, gain, taps, bias, rw, rb, ew, eb, rate,
    out_e, out_q, entry_v, valve_v, ow_v, tokens_v, gain_v, rows_v, rw_v, ew_v,
    taps_v, bias_v, rb_v, eb_v, rate_v, sems,
):
    x, c = idx[0], idx[1]
    eighth = 2 * x + c
    moves = (
        (taps, taps_v), (bias, bias_v), (rb, rb_v), (eb, eb_v), (rate, rate_v), (rw, rw_v),
        (ew, ew_v), (entry, entry_v), (valve, valve_v), (ow, ow_v), (tokens, tokens_v),
        (gain, gain_v),
    )
    copies = [pltpu.make_async_copy(a, b, sems.at[k]) for k, (a, b) in enumerate(moves)]
    for copy in copies:
        copy.start()
    for copy in copies:
        copy.wait()
    out_e[0:HALF] = entry_v[pl.ds(pl.multiple_of(c * HALF, HALF), HALF), :]
    out_e[HALF : HALF + 128] = jnp.where(c == 0, rw_v[0], ew_v[0])
    rows = jnp.concatenate([taps_v[...], bias_v[...], rb_v[...], eb_v[...], rate_v[...]], axis=0)
    rows_v[...] = rows
    high = rows.astype(BF16).astype(F32)
    rest = rows - high
    middle = rest.astype(BF16).astype(F32)
    low = rest - middle
    out_e[HALF + 128 :] = jnp.concatenate(
        [high, middle, low, jnp.zeros_like(low)], axis=0
    ).astype(BF16)
    out_q[0:256] = valve_v[pl.ds(pl.multiple_of(eighth * 256, 256), 256), :]
    rows = ow_v[pl.ds(pl.multiple_of(eighth * 16, 16), 16), :]
    for n in range(16):
        out_q[256 + n * 16 : 272 + n * 16] = rows[:, n * 128 : n * 128 + 128]


def join_kernel(idx, q1, q2, q3, out):
    for k, q in enumerate((q1, q2, q3)):
        out[k * 512 : k * 512 + 512] = q[...]


def norm_kernel(idx, t0, t1, t2, t3, gain, xn, halo):
    y = idx[3]
    g = gain[...]
    for piece, source in zip((t0, t1, t2, t3), SOURCES):
        slot = pl.multiple_of(((y + source) % 4) * 16, 16)
        for s in range(4):
            v = piece[s].astype(F32)
            scale = lax.rsqrt(jnp.mean(v * v, axis=-1, keepdims=True) + EPS)
            n = (v * scale * g).astype(BF16)
            xn[0, s, pl.ds(slot, 16), :] = n[:, :HALF]
            xn[1, s, pl.ds(slot, 16), :] = n[:, HALF:]
    for k in range(2):
        tails = [xn[k, s, 48:64, :].astype(F32)[12:16] for s in range(4)]
        halo[k] = jnp.concatenate(tails, axis=0).astype(BF16)


def both_halves(own, idx):
    c = idx[1]
    first = own[pl.ds(pl.multiple_of(c * HALF, HALF), HALF), :]
    second = own[pl.ds(pl.multiple_of((1 - c) * HALF, HALF), HALF), :]
    return first, second


def gates_kernel(
    idx, xn, halo, entry, own_rows, rw, ew,
    a1, a2, a3, b1, b2, b3,
    hloc, acum, ends, total,
    pad,
):
    c, z = idx[1], idx[2]
    lhs_a = jnp.concatenate([xn[c].reshape(256, HALF), halo[c]], axis=0)
    lhs_b = jnp.concatenate([xn[1 - c].reshape(256, HALF), halo[1 - c]], axis=0)
    own_a, own_b = both_halves(entry, idx)
    near, far = (a1, a2, a3), (b1, b2, b3)
    us = []
    for wa, wb in (
        ((own_a, a1[0:HALF]), (own_b, b1[0:HALF])),
        ((a2[0:HALF], a3[0:HALF]), (b2[0:HALF], b3[0:HALF])),
    ):
        u = jnp.dot(lhs_a, jnp.concatenate(wa, axis=1), preferred_element_type=F32)
        u = u + jnp.dot(lhs_b, jnp.concatenate(wb, axis=1), preferred_element_type=F32)
        u = u.astype(BF16).astype(F32)
        us += [u[:, :128], u[:, 128:]]
    for j in range(4):
        u = us[j]
        if j == 0:
            p = own_rows[...]
            rwj, ewj = rw[0], ew[0]
        else:
            q = near[j - 1][HALF + 128 :].astype(F32)
            p = q[0:8] + q[8:16] + q[16:24]
            mine, other = near[j - 1][HALF : HALF + 128], far[j - 1][HALF : HALF + 128]
            rwj = jnp.where(c == 0, mine, other)
            ewj = jnp.where(c == 0, other, mine)
        for s in range(4):
            for half in range(2):
                row = s * 64 + half * 32
                pad[j, pl.ds(24 + half * 4 + s, 32, stride=8), :] = u[row : row + 32]
            for k in range(3):
                pad[j, k * 8 + s : k * 8 + s + 1, :] = u[257 + s * 4 + k : 258 + s * 4 + k]
        for k in range(3):
            pad[j, k * 8 + 4 : k * 8 + 8, :] = pad[j, (32 + k) * 8 : (32 + k) * 8 + 4, :]
        conv = p[4:5] + pad[j, 0:256, :] * p[0:1]
        for k in range(1, 4):
            conv = conv + pad[j, k * 8 : k * 8 + 256, :] * p[k : k + 1]
        conv16 = conv.astype(BF16)
        conv = conv16.astype(F32)
        g = jnp.dot(conv16, jnp.concatenate([rwj, ewj], axis=1), preferred_element_type=F32)
        r = jax.nn.sigmoid(g[:, :128] + p[5:6])
        e = jax.nn.sigmoid(g[:, 128:] + p[6:7])
        log_decay = -GATE_POWER * r * p[7:8]
        decay = jnp.exp(log_decay)
        acum[j] = decay
        hloc[j] = jnp.sqrt(-jnp.tanh(log_decay) * (1.0 + decay * decay)) * (e * conv)
    h = [jnp.zeros((8, 128), F32) for _ in range(4)]
    a = [jnp.ones((8, 128), F32) for _ in range(4)]
    for t in range(32):
        for j in range(4):
            step = acum[j, t * 8 : t * 8 + 8, :]
            h[j] = step * h[j] + hloc[j, t * 8 : t * 8 + 8, :]
            a[j] = step * a[j]
            hloc[j, t * 8 : t * 8 + 8, :] = h[j]
            acum[j, t * 8 : t * 8 + 8, :] = a[j]
    for j in range(4):
        ends[0, j] = a[j]
        ends[1, j] = h[j]
        shard = (z + SOURCES[j]) % 4
        total[0, shard] = a[j][0:4] * a[j][4:8]
        total[1, shard] = a[j][4:8] * h[j][0:4] + h[j][4:8]


def prepare_kernel(idx, xn, valve, ow, g0, g1, g2, g3, f0, f1, f2, f3, silu, wo, wv):
    x, c = idx[0], idx[1]
    wv[:, 0:128] = valve[...]
    wo[0:128] = ow[...]
    for m, (mine, other) in enumerate(((g0, f0), (g1, f1), (g2, f2), (g3, f3))):
        for core, piece in ((c, mine), (1 - c, other)):
            eighth = ((x + SOURCES[m]) % 4) * 2 + core
            for j in range(1, 4):
                top = (j - 1) * 512
                wv[pl.ds(pl.multiple_of(eighth * 256, 256), 256), j * 128 : j * 128 + 128] = piece[
                    top : top + 256
                ]
                row = pl.multiple_of(j * 128 + eighth * 16, 16)
                for n in range(16):
                    wo[pl.ds(row, 16), n * 128 : n * 128 + 128] = piece[
                        top + 256 + n * 16 : top + 272 + n * 16
                    ]
    u = jnp.dot(xn[0].reshape(256, HALF), wv[0:HALF], preferred_element_type=F32)
    u = u + jnp.dot(xn[1].reshape(256, HALF), wv[HALF:], preferred_element_type=F32)
    u = u.astype(BF16).astype(F32)
    silu[...] = u * jax.nn.sigmoid(u)


def output_kernel(
    idx, hloc, acum, ends, entering, silu, wo, out0, out1, out2, out3, hs, gated
):
    z, y = idx[2], idx[3]
    for j in range(4):
        first = entering[(z + SOURCES[j]) % 4]
        second = ends[1, j, 0:4, :] + ends[0, j, 0:4, :] * first
        state = jnp.concatenate([first, second], axis=0)
        h = hloc[j].reshape(32, 8, 128) + acum[j].reshape(32, 8, 128) * state[None]
        hs[j] = h.reshape(256, 128)
        for s in range(4):
            for half in range(2):
                row = s * 64 + half * 32
                hidden = hs[j, pl.ds(half * 4 + s, 32, stride=8), :]
                gated[s, half * 32 : half * 32 + 32, j * 128 : j * 128 + 128] = (
                    hidden * silu[row : row + 32, j * 128 : j * 128 + 128]
                ).astype(BF16)
    rows = []
    for d in (0, 1, 3, 2):
        slot = pl.multiple_of(((y + d) % 4) * 16, 16)
        rows += [gated[s, pl.ds(slot, 16), :] for s in range(4)]
    mixed = jnp.dot(jnp.concatenate(rows, axis=0), wo[...], preferred_element_type=F32)
    out0[...] = mixed[0:64].reshape(4, 16, 2048)
    for k, out in enumerate((out1, out2, out3), 1):
        out[...] = mixed[k * 64 : k * 64 + 64].reshape(4, 16, 2048).astype(BF16)


def mix_kernel(idx, own, r1, r2, r3, out):
    total = own[...] + r1[...].astype(F32) + r2[...].astype(F32) + r3[...].astype(F32)
    out[...] = total.astype(BF16)


def after(earlier, later):
    return earlier[0] * later[0], later[0] * earlier[1] + later[1]


def level_kernel(idx, total, other, *rest, position, mirrored, first, last):
    state = None if first else rest[0]
    out = rest if first else rest[1:]
    place = idx[position]
    upper = (place >= 2) if mirrored else (place % 2 == 1)
    mine = (total[0], total[1])
    theirs = (other[0], other[1])
    if first:
        new = [jnp.where(upper, theirs[0], 1.0), jnp.where(upper, theirs[1], 0.0)]
    else:
        old = (state[0], state[1])
        new = [jnp.where(upper, n, o) for n, o in zip(after(theirs, old), old)]
    if last:
        out[0][...] = new[1]
        return
    out[0][0], out[0][1] = new
    earlier = [jnp.where(upper, t, m) for t, m in zip(theirs, mine)]
    later = [jnp.where(upper, m, t) for t, m in zip(theirs, mine)]
    out[1][0], out[1][1] = after(earlier, later)


def enter(total, idx):
    levels = (("z", False), ("z", True), ("c", False), ("x", False), ("x", True))
    state = None
    for k, (axis, mirrored) in enumerate(levels):
        size = lax.axis_size(axis)
        partner = [(i, size - 1 - i if mirrored else i ^ 1) for i in range(size)]
        other = lax.ppermute(total, axis, partner)
        first, last = k == 0, k == len(levels) - 1
        kernel = functools.partial(
            level_kernel,
            position=SP_TP.index(axis),
            mirrored=mirrored,
            first=first,
            last=last,
        )
        pair = ((2, 4, 4, 128), F32)
        outs = [((4, 4, 128), F32)] if last else [pair, pair]
        ins = (total, other) if first else (total, other, state)
        state, *left = call(kernel, idx, ins, outs)
        total = left[0] if left else None
    return state


def per_device(
    tokens,
    norm_gain,
    entry_projection,
    valve_projection,
    filter_taps,
    conv_bias,
    recur_weight,
    recur_bias,
    entry_weight,
    entry_bias,
    forget_rate,
    output_weight,
):
    idx = jnp.stack([lax.axis_index(a) for a in SP_TP]).astype(jnp.int32)
    vector = lambda a: a.reshape(1, -1)
    small = (
        filter_taps,
        vector(conv_bias),
        recur_weight,
        vector(recur_bias),
        entry_weight,
        vector(entry_bias),
        vector(forget_rate),
    )
    pieces = spread(tokens, "y")
    gate = ((1, 128, 128), BF16)
    message, eighths, entry, valve, ow, own_tokens, gain, rows, rw, ew = call(
        fetch_kernel,
        idx,
        (entry_projection, valve_projection, output_weight, tokens, vector(norm_gain), *small),
        [
            ((HALF + 160, 128), BF16), ((512, 128), BF16), ((2048, 128), BF16),
            ((2048, 128), BF16), ((128, 2048), BF16), ((4, 16, 2048), BF16), ((1, 2048), F32),
            ((8, 128), F32), gate, gate,
        ],
        scratch=[pltpu.VMEM((4, 128), F32)]
        + [pltpu.VMEM((1, 128), F32)] * 4
        + [pltpu.SemaphoreType.DMA((12,))],
        far=12,
    )
    quarters = spread(eighths, "z")
    entry_near = spread(message, "z")
    (joined,) = call(join_kernel, idx, quarters, [((1536, 128), BF16)])
    gathered = [joined] + spread(joined, "x")
    xn, halo = call(
        norm_kernel,
        idx,
        (own_tokens, *pieces, gain),
        [((2, 4, 64, HALF), BF16), ((2, 16, HALF), BF16)],
    )
    stretches = 32
    halo_in = lax.ppermute(halo, ("x", "c", "z"), [(i, i + 1) for i in range(stretches - 1)])
    entry_far = swap_cores(entry_near)
    gathered_far = swap_cores(gathered)
    hloc, acum, ends, total = call(
        gates_kernel,
        idx,
        (xn, halo_in, entry, rows, rw, ew, *entry_near, *entry_far),
        [((4, 256, 128), F32), ((4, 256, 128), F32), ((2, 4, 8, 128), F32), ((2, 4, 4, 128), F32)],
        scratch=[pltpu.VMEM((4, 280, 128), F32)],
    )
    entering = enter(total, idx)
    silu, wo = call(
        prepare_kernel,
        idx,
        (xn, valve, ow, *gathered, *gathered_far),
        [((256, 512), F32), ((512, 2048), BF16)],
        scratch=[pltpu.VMEM((2048, 512), BF16)],
    )
    own, *parts = call(
        output_kernel,
        idx,
        (hloc, acum, ends, entering, silu, wo),
        [((4, 16, 2048), F32)] + [((4, 16, 2048), BF16)] * 3,
        scratch=[pltpu.VMEM((4, 256, 128), F32), pltpu.VMEM((4, 64, 512), BF16)],
    )
    parts = [shift(p, "y", by) for p, by in zip(parts, SHIFTS)]
    (mixed,) = call(mix_kernel, idx, (own, *parts), [((4, 16, 2048), BF16)], to_hbm=True)
    return mixed


def solution(mesh):
    finer = Mesh(mesh.devices.reshape(4, 2, 4, 4), SP_TP)
    placed = (
        P(None, SP_TP, None),
        P(),
        P(None, TP),
        P(None, TP),
        P(None, TP),
        P(TP),
        P(TP, None, None),
        P(TP),
        P(TP, None, None),
        P(TP),
        P(TP),
        P(TP, None),
    )

    return jax.shard_map(
        per_device, mesh=finer, in_specs=placed, out_specs=P(None, SP_TP, None), check_vma=False
    )
```

profile of v0, /device:TPU:0, one launch (start us, length us, event | category | flops | bytes accessed | tf_op | source)
XLA Modules:
  0.0 89.9 jit_solution(2051747191142156461)
XLA Ops:
  0.0 1.7 %collective-permute-start = (bf16[4,16,2048]{2,1,0:T(8,128)(2,1)}, bf16[4,16,2048]{2,1,0:T(8,128)(2,1)S(1)}, u32[]{:S(2)}, u32[]{:S(2)}) collective-permute-start(bf16[4,16,2048]{2,1,0:T(8,128)(2,1)} %tokens.1), channel_id=1, source_target_pairs={{0,1},{1,2},{2,3},{3,0},{4,5},{5,6},{6,7},{7,4},{8,9},{9,10},{10,1... | collective-permute-start | bytes 786440 | tf_op jit(solution)/shard_map/ppermute | solution.py:25
  1.8 2.2 %shard_map.118 = (bf16[1184,128]{1,0:T(8,128)(2,1)S(1)}, bf16[512,128]{1,0:T(8,128)(2,1)S(1)}, bf16[2048,128]{1,0:T(8,128)(2,1)S(1)}, bf16[2048,128]{1,0:T(8,128...) custom-call(s32[4]{0:T(128)S(1)} %pad_add_fusion.idx, ...), custom_call_target="tpu_custom_call" | custom-call | tf_op jit(solution)/shard_map/pallas_call | solution.py:40
  4.0 2.0 %collective-permute-start.15 = (bf16[512,128]{1,0:T(8,128)(2,1)S(1)}, bf16[512,128]{1,0:T(8,128)(2,1)S(1)}, u32[]{:S(2)}, u32[]{:S(2)}) collective-permute-start(bf16[512,128]{1,0:T(8,128)(2,1)S(1)} %get-tuple-element.58), channel_id=1, source_target_pairs={{0,4},{4,8},{8,12},{12,0},{1,5},{5,9},{9,13},{13,1},{2,6},{6,10},{... | collective-permute-start | bytes 393224 | tf_op jit(solution)/shard_map/ppermute | solution.py:25
  6.0 2.2 %collective-permute-start.16 = (bf16[512,128]{1,0:T(8,128)(2,1)S(1)}, bf16[512,128]{1,0:T(8,128)(2,1)S(1)}, u32[]{:S(2)}, u32[]{:S(2)}) collective-permute-start(bf16[512,128]{1,0:T(8,128)(2,1)S(1)} %get-tuple-element.58), channel_id=1, source_target_pairs={{0,12},{4,0},{8,4},{12,8},{1,13},{5,1},{9,5},{13,9},{2,14},{6,2},{... | collective-permute-start | bytes 393224 | tf_op jit(solution)/shard_map/ppermute | solution.py:25
  8.2 1.8 %collective-permute-start.17 = (bf16[512,128]{1,0:T(8,128)(2,1)S(1)}, bf16[512,128]{1,0:T(8,128)(2,1)S(1)}, u32[]{:S(2)}, u32[]{:S(2)}) collective-permute-start(bf16[512,128]{1,0:T(8,128)(2,1)S(1)} %get-tuple-element.58), channel_id=1, source_target_pairs={{0,8},{4,12},{8,0},{12,4},{1,9},{5,13},{9,1},{13,5},{2,10},{6,14},... | collective-permute-start | bytes 393224 | tf_op jit(solution)/shard_map/ppermute | solution.py:25
  10.0 1.0 %collective-permute-start.4 = (bf16[1184,128]{1,0:T(8,128)(2,1)S(1)}, bf16[1184,128]{1,0:T(8,128)(2,1)S(1)}, u32[]{:S(2)}, u32[]{:S(2)}) collective-permute-start(bf16[1184,128]{1,0:T(8,128)(2,1)S(1)} %get-tuple-element.43), channel_id=1, source_target_pairs={{0,4},{4,8},{8,12},{12,0},{1,5},{5,9},{9,13},{13,1},{2,6},{6,10},{... | collective-permute-start | bytes 909320 | tf_op jit(solution)/shard_map/ppermute | solution.py:25
  11.0 0.3 collective-permute-done.15.q1
  11.3 2.7 %collective-permute-start.5 = (bf16[1184,128]{1,0:T(8,128)(2,1)S(1)}, bf16[1184,128]{1,0:T(8,128)(2,1)S(1)}, u32[]{:S(2)}, u32[]{:S(2)}) collective-permute-start(bf16[1184,128]{1,0:T(8,128)(2,1)S(1)} %get-tuple-element.43), channel_id=1, source_target_pairs={{0,12},{4,0},{8,4},{12,8},{1,13},{5,1},{9,5},{13,9},{2,14},{6,2},{... | collective-permute-start | bytes 909320 | tf_op jit(solution)/shard_map/ppermute | solution.py:25
  14.0 1.7 %collective-permute-start.1 = (bf16[4,16,2048]{2,1,0:T(8,128)(2,1)}, bf16[4,16,2048]{2,1,0:T(8,128)(2,1)S(1)}, u32[]{:S(2)}, u32[]{:S(2)}) collective-permute-start(bf16[4,16,2048]{2,1,0:T(8,128)(2,1)} %tokens.1), channel_id=1, source_target_pairs={{0,3},{1,0},{2,1},{3,2},{4,7},{5,4},{6,5},{7,6},{8,11},{9,8},{10,9... | collective-permute-start | bytes 786440 | tf_op jit(solution)/shard_map/ppermute | solution.py:25
  15.7 0.5 collective-permute-done.17.q3
  16.3 2.9 %collective-permute-start.2 = (bf16[4,16,2048]{2,1,0:T(8,128)(2,1)}, bf16[4,16,2048]{2,1,0:T(8,128)(2,1)S(1)}, u32[]{:S(2)}, u32[]{:S(2)}) collective-permute-start(bf16[4,16,2048]{2,1,0:T(8,128)(2,1)} %tokens.1), channel_id=1, source_target_pairs={{0,2},{1,3},{2,0},{3,1},{4,6},{5,7},{6,4},{7,5},{8,10},{9,11},{10,... | collective-permute-start | bytes 786440 | tf_op jit(solution)/shard_map/ppermute | solution.py:25
  19.2 1.6 %collective-permute-start.6 = (bf16[1184,128]{1,0:T(8,128)(2,1)S(1)}, bf16[1184,128]{1,0:T(8,128)(2,1)S(1)}, u32[]{:S(2)}, u32[]{:S(2)}) collective-permute-start(bf16[1184,128]{1,0:T(8,128)(2,1)S(1)} %get-tuple-element.43), channel_id=1, source_target_pairs={{0,8},{4,12},{8,0},{12,4},{1,9},{5,13},{9,1},{13,5},{2,10},{6,14},... | collective-permute-start | bytes 909320 | tf_op jit(solution)/shard_map/ppermute | solution.py:25
  20.8 0.6 shard_map.126.g0
  21.3 2.1 %collective-permute-done.1.t2 = bf16[4,16,2048]{2,1,0:T(8,128)(2,1)S(1)} collective-permute-done((bf16[4,16,2048]{2,1,0:T(8,128)(2,1)}, bf16[4,16,2048]{2,1,0:T(8,128)(2,1)S(1)}, u32[]{:S(2)}, u32[]{:S(2)}) %collective-permute-start.1) | collective-permute-done | bytes 262176 | tf_op jit(solution)/shard_map/ppermute | solution.py:25
  23.4 1.5 %collective-permute-start.18 = (bf16[1536,128]{1,0:T(8,128)(2,1)S(1)}, bf16[1536,128]{1,0:T(8,128)(2,1)S(1)}, u32[]{:S(2)}, u32[]{:S(2)}) collective-permute-start(bf16[1536,128]{1,0:T(8,128)(2,1)S(1)} %shard_map.126.g0), channel_id=1, source_target_pairs={{0,32},{32,64},{64,96},{96,0},{1,33},{33,65},{65,97},{97,1},{2,34}... | collective-permute-start | bytes 1179656 | tf_op jit(solution)/shard_map/ppermute | solution.py:25
  24.9 2.3 %collective-permute-start.19 = (bf16[1536,128]{1,0:T(8,128)(2,1)S(1)}, bf16[1536,128]{1,0:T(8,128)(2,1)S(1)}, u32[]{:S(2)}, u32[]{:S(2)}) collective-permute-start(bf16[1536,128]{1,0:T(8,128)(2,1)S(1)} %shard_map.126.g0), channel_id=1, source_target_pairs={{0,96},{32,0},{64,32},{96,64},{1,97},{33,1},{65,33},{97,65},{2,98}... | collective-permute-start | bytes 1179656 | tf_op jit(solution)/shard_map/ppermute | solution.py:25
  27.2 1.3 %collective-permute-start.20 = (bf16[1536,128]{1,0:T(8,128)(2,1)S(1)}, bf16[1536,128]{1,0:T(8,128)(2,1)S(1)}, u32[]{:S(2)}, u32[]{:S(2)}) collective-permute-start(bf16[1536,128]{1,0:T(8,128)(2,1)S(1)} %shard_map.126.g0), channel_id=1, source_target_pairs={{0,64},{32,96},{64,0},{96,32},{1,65},{33,97},{65,1},{97,33},{2,66}... | collective-permute-start | bytes 1179656 | tf_op jit(solution)/shard_map/ppermute | solution.py:25
  28.4 1.0 %shard_map.119 = (bf16[2,4,64,1024]{3,2,1,0:T(8,128)(2,1)S(1)}, bf16[2,16,1024]{2,1,0:T(8,128)(2,1)S(1)}) custom-call(s32[4]{0:T(128)S(1)} %pad_add_fusion.idx, bf16[4,16,2048]{2,1,0:T(8,128)(2,1)S(1)} %get-tuple-element.35.t0, bf16[4,16,2048]{2,1,0:T(8,128)(2,1)S(1)} %collective-permute-done.t1, bf16[4,16,2048]{2,1,0:T(8,128)(2,1)S(1)} %collective-permute-done.1.t2, ...), custom_call_target="tpu_custom_call" | custom-call | tf_op jit(solution)/shard_map/pallas_call | solution.py:40
  29.4 3.3 %collective-permute-start.3 = (bf16[2,16,1024]{2,1,0:T(8,128)(2,1)S(1)}, bf16[2,16,1024]{2,1,0:T(8,128)(2,1)S(1)}, u32[]{:S(2)}, u32[]{:S(2)}) collective-permute-start(bf16[2,16,1024]{2,1,0:T(8,128)(2,1)S(1)} %get-tuple-element.38), channel_id=1, source_target_pairs={{0,4},{4,8},{8,12},{12,16},{16,20},{20,24},{24,28},{28,32},{32,36}... | collective-permute-start | bytes 196616 | tf_op jit(solution)/shard_map/ppermute | solution.py:342
  32.8 1.8 %collective-permute-done.3.halo = bf16[2,16,1024]{2,1,0:T(8,128)(2,1)S(1)} collective-permute-done((bf16[2,16,1024]{2,1,0:T(8,128)(2,1)S(1)}, bf16[2,16,1024]{2,1,0:T(8,128)(2,1)S(1)}, u32[]{:S(2)}, u32[]{:S(2)}) %collective-permute-start.3) | collective-permute-done | bytes 65568 | tf_op jit(solution)/shard_map/ppermute | solution.py:342
  34.6 2.1 %collective-permute-start.8 = (bf16[1184,128]{1,0:T(8,128)(2,1)S(1)}, bf16[1184,128]{1,0:T(8,128)(2,1)S(1)}, u32[]{:S(2)}, u32[]{:S(2)}) collective-permute-start(bf16[1184,128]{1,0:T(8,128)(2,1)S(1)} %collective-permute-done.5.a2), channel_id=1, source_target_pairs={{0,16},{16,0},{1,17},{17,1},{2,18},{18,2},{3,19},{19,3},{4,20},{20... | collective-permute-start | bytes 909320 | tf_op jit(solution)/shard_map/ppermute | solution.py:25
  36.7 4.8 %collective-permute-done.19.g2 = bf16[1536,128]{1,0:T(8,128)(2,1)S(1)} collective-permute-done((bf16[1536,128]{1,0:T(8,128)(2,1)S(1)}, bf16[1536,128]{1,0:T(8,128)(2,1)S(1)}, u32[]{:S(2)}, u32[]{:S(2)}) %collective-permute-start.19) | collective-permute-done | bytes 393248 | tf_op jit(solution)/shard_map/ppermute | solution.py:25
  41.5 0.5 collective-permute-start.23
  42.1 0.4 collective-permute-start.9
  42.6 2.2 %collective-permute-done.9.b3 = bf16[1184,128]{1,0:T(8,128)(2,1)S(1)} collective-permute-done((bf16[1184,128]{1,0:T(8,128)(2,1)S(1)}, bf16[1184,128]{1,0:T(8,128)(2,1)S(1)}, u32[]{:S(2)}, u32[]{:S(2)}) %collective-permute-start.9) | collective-permute-done | bytes 303136 | tf_op jit(solution)/shard_map/ppermute | solution.py:25
  44.8 2.0 %shard_map.120 = (f32[4,256,128]{2,1,0:T(8,128)S(1)}, f32[4,256,128]{2,1,0:T(8,128)S(1)}, f32[2,4,8,128]{3,2,1,0:T(8,128)S(1)}, f32[2,4,4,128]{3,2,1,0:T(4,128)S(1)}) custom-call(s32[4]{0:T(128)S(1)} %pad_add_fusion.idx, bf16[2,4,64,1024]{3,2,1,0:T(8,128)(2,1)S(1)} %get-tuple-element.37.xn, bf16[2,16,1024]{2,1,0:T(8,128)(2,1)S(1)} %collective-permute-done.3.halo, ...), custom_call_target="tpu_custom_call" | custom-call | tf_op jit(solution)/shard_map/pallas_call | solution.py:40
  47.0 3.7 %collective-permute-done.10.other = f32[2,4,4,128]{3,2,1,0:T(4,128)S(1)} collective-permute-done((f32[2,4,4,128]{3,2,1,0:T(4,128)S(1)}, f32[2,4,4,128]{3,2,1,0:T(4,128)S(1)}, u32[]{:S(2)}, u32[]{:S(2)}) %collective-permute-start.10) | collective-permute-done | bytes 16416 | tf_op jit(solution)/shard_map/ppermute | solution.py:273
  50.7 0.6 shard_map.121
  51.2 1.4 %collective-permute-start.11 = (f32[2,4,4,128]{3,2,1,0:T(4,128)S(1)}, f32[2,4,4,128]{3,2,1,0:T(4,128)S(1)}, u32[]{:S(2)}, u32[]{:S(2)}) collective-permute-start(f32[2,4,4,128]{3,2,1,0:T(4,128)S(1)} %get-tuple-element.48.total), channel_id=1, source_target_pairs={{0,12},{4,8},{8,4},{12,0},{1,13},{5,9},{9,5},{13,1},{2,14},{6,10},... | collective-permute-start | bytes 49160 | tf_op jit(solution)/shard_map/ppermute | solution.py:273
  52.6 3.6 %collective-permute-done.11.other = f32[2,4,4,128]{3,2,1,0:T(4,128)S(1)} collective-permute-done((f32[2,4,4,128]{3,2,1,0:T(4,128)S(1)}, f32[2,4,4,128]{3,2,1,0:T(4,128)S(1)}, u32[]{:S(2)}, u32[]{:S(2)}) %collective-permute-start.11) | collective-permute-done | bytes 16416 | tf_op jit(solution)/shard_map/ppermute | solution.py:273
  56.3 0.6 shard_map.122
  56.9 1.2 %collective-permute-done.12.other = f32[2,4,4,128]{3,2,1,0:T(4,128)S(1)} collective-permute-done((f32[2,4,4,128]{3,2,1,0:T(4,128)S(1)}, f32[2,4,4,128]{3,2,1,0:T(4,128)S(1)}, u32[]{:S(2)}, u32[]{:S(2)}) %collective-permute-start.12) | collective-permute-done | bytes 16416 | tf_op jit(solution)/shard_map/ppermute | solution.py:273
  58.1 0.6 shard_map.123
  58.7 1.6 %collective-permute-start.13 = (f32[2,4,4,128]{3,2,1,0:T(4,128)S(1)}, f32[2,4,4,128]{3,2,1,0:T(4,128)S(1)}, u32[]{:S(2)}, u32[]{:S(2)}) collective-permute-start(f32[2,4,4,128]{3,2,1,0:T(4,128)S(1)} %get-tuple-element.52.total), channel_id=1, source_target_pairs={{0,32},{32,0},{64,96},{96,64},{1,33},{33,1},{65,97},{97,65},{2,34}... | collective-permute-start | bytes 49160 | tf_op jit(solution)/shard_map/ppermute | solution.py:273
  60.3 2.2 %collective-permute-done.13.other = f32[2,4,4,128]{3,2,1,0:T(4,128)S(1)} collective-permute-done((f32[2,4,4,128]{3,2,1,0:T(4,128)S(1)}, f32[2,4,4,128]{3,2,1,0:T(4,128)S(1)}, u32[]{:S(2)}, u32[]{:S(2)}) %collective-permute-start.13) | collective-permute-done | bytes 16416 | tf_op jit(solution)/shard_map/ppermute | solution.py:273
  62.5 0.6 shard_map.124
  63.0 3.7 %collective-permute-start.14 = (f32[2,4,4,128]{3,2,1,0:T(4,128)S(1)}, f32[2,4,4,128]{3,2,1,0:T(4,128)S(1)}, u32[]{:S(2)}, u32[]{:S(2)}) collective-permute-start(f32[2,4,4,128]{3,2,1,0:T(4,128)S(1)} %get-tuple-element.54.total), channel_id=1, source_target_pairs={{0,96},{32,64},{64,32},{96,0},{1,97},{33,65},{65,33},{97,1},{2,98}... | collective-permute-start | bytes 49160 | tf_op jit(solution)/shard_map/ppermute | solution.py:273
  66.8 1.7 %collective-permute-done.14.other = f32[2,4,4,128]{3,2,1,0:T(4,128)S(1)} collective-permute-done((f32[2,4,4,128]{3,2,1,0:T(4,128)S(1)}, f32[2,4,4,128]{3,2,1,0:T(4,128)S(1)}, u32[]{:S(2)}, u32[]{:S(2)}) %collective-permute-start.14) | collective-permute-done | bytes 16416 | tf_op jit(solution)/shard_map/ppermute | solution.py:273
  68.5 0.5 shard_map.125.entering
  69.1 2.0 %shard_map.127 = (f32[256,512]{1,0:T(8,128)S(1)}, bf16[512,2048]{1,0:T(8,128)(2,1)S(1)}) custom-call(s32[4]{0:T(128)S(1)} %pad_add_fusion.idx, bf16[2,4,64,1024]{3,2,1,0:T(8,128)(2,1)S(1)} %get-tuple-element.37.xn, bf16[2048,128]{1,0:T(8,128)(2,1)S(1)} %get-tuple-element.56.valve, bf16[128,2048]{1,0:T(8,128)(2,1)S(1)} %get-tuple-element.57.ow, ...), custom_call_target="tpu_custom_call" | custom-call | tf_op jit(solution)/shard_map/pallas_call | solution.py:40
  71.1 1.5 %shard_map.128 = (f32[4,16,2048]{2,1,0:T(8,128)S(1)}, bf16[4,16,2048]{2,1,0:T(8,128)(2,1)S(1)}, bf16[4,16,2048]{2,1,0:T(8,128)(2,1)S(1)}, bf16[4,16,2048]{2,1,0:T(8,128)(2,1)S(1)}) custom-call(s32[4]{0:T(128)S(1)} %pad_add_fusion.idx, f32[4,256,128]{2,1,0:T(8,128)S(1)} %get-tuple-element.44.hloc, f32[4,256,128]{2,1,0:T(8,128)S(1)} %get-tuple-element.45.acum, ...), custom_call_target="tpu_custom_call" | custom-call | tf_op jit(solution)/shard_map/pallas_call | solution.py:40
  72.6 4.4 %collective-permute-start.25 = (bf16[4,16,2048]{2,1,0:T(8,128)(2,1)S(1)}, bf16[4,16,2048]{2,1,0:T(8,128)(2,1)S(1)}, u32[]{:S(2)}, u32[]{:S(2)}) collective-permute-start(bf16[4,16,2048]{2,1,0:T(8,128)(2,1)S(1)} %get-tuple-element.62), channel_id=1, source_target_pairs={{0,1},{1,2},{2,3},{3,0},{4,5},{5,6},{6,7},{7,4},{8,9},{9,10},{10,1... | collective-permute-start | bytes 786440 | tf_op jit(solution)/shard_map/ppermute | solution.py:25
  77.0 0.2 collective-permute-start.26
  77.2 1.9 %collective-permute-start.27 = (bf16[4,16,2048]{2,1,0:T(8,128)(2,1)S(1)}, bf16[4,16,2048]{2,1,0:T(8,128)(2,1)S(1)}, u32[]{:S(2)}, u32[]{:S(2)}) collective-permute-start(bf16[4,16,2048]{2,1,0:T(8,128)(2,1)S(1)} %get-tuple-element.64), channel_id=1, source_target_pairs={{0,2},{1,3},{2,0},{3,1},{4,6},{5,7},{6,4},{7,5},{8,10},{9,11},{10,... | collective-permute-start | bytes 786440 | tf_op jit(solution)/shard_map/ppermute | solution.py:25
  79.1 4.5 %collective-permute-done.25.r1 = bf16[4,16,2048]{2,1,0:T(8,128)(2,1)S(1)} collective-permute-done((bf16[4,16,2048]{2,1,0:T(8,128)(2,1)S(1)}, bf16[4,16,2048]{2,1,0:T(8,128)(2,1)S(1)}, u32[]{:S(2)}, u32[]{:S(2)}) %collective-permute-start.25) | collective-permute-done | bytes 262176 | tf_op jit(solution)/shard_map/ppermute | solution.py:25
  83.7 2.2 %collective-permute-done.26.r2 = bf16[4,16,2048]{2,1,0:T(8,128)(2,1)S(1)} collective-permute-done((bf16[4,16,2048]{2,1,0:T(8,128)(2,1)S(1)}, bf16[4,16,2048]{2,1,0:T(8,128)(2,1)S(1)}, u32[]{:S(2)}, u32[]{:S(2)}) %collective-permute-start.26) | collective-permute-done | bytes 262176 | tf_op jit(solution)/shard_map/ppermute | solution.py:25
  85.8 2.7 %collective-permute-done.27.r3 = bf16[4,16,2048]{2,1,0:T(8,128)(2,1)S(1)} collective-permute-done((bf16[4,16,2048]{2,1,0:T(8,128)(2,1)S(1)}, bf16[4,16,2048]{2,1,0:T(8,128)(2,1)S(1)}, u32[]{:S(2)}, u32[]{:S(2)}) %collective-permute-start.27) | collective-permute-done | bytes 262176 | tf_op jit(solution)/shard_map/ppermute | solution.py:25
  88.5 1.4 %shard_map.129 = bf16[4,16,2048]{2,1,0:T(8,128)(2,1)} custom-call(s32[4]{0:T(128)S(1)} %pad_add_fusion.idx, f32[4,16,2048]{2,1,0:T(8,128)S(1)} %get-tuple-element.61.own, bf16[4,16,2048]{2,1,0:T(8,128)(2,1)S(1)} %collective-permute-done.25.r1, bf16[4,16,2048]{2,1,0:T(8,128)(2,1)S(1)} %collective-permute-done.26.r2, ...), custom_call_target="tpu_custom_call" | custom-call | tf_op jit(solution)/shard_map/pallas_call | solution.py:40
  (21 shorter events, 0.5 us)
Async XLA Ops:
  0.0 19.2 %collective-permute-start = (bf16[4,16,2048]{2,1,0:T(8,128)(2,1)}, bf16[4,16,2048]{2,1,0:T(8,128)(2,1)S(1)}, u32[]{:S(2)}, u32[]{:S(2)}) collective-permute-start(bf16[4,16,2048]{2,1,0:T(8,128)(2,1)} %tokens.1), channel_id=1, source_target_pairs={{0,1},{1,2},{2,3},{3,0},{4,5},{5,6},{6,7},{7,4},{8,9},{9,10},{10,1... | collective-permute-start | bytes 786440 | tf_op jit(solution)/shard_map/ppermute | solution.py:25
  4.0 7.3 %collective-permute-start.15 = (bf16[512,128]{1,0:T(8,128)(2,1)S(1)}, bf16[512,128]{1,0:T(8,128)(2,1)S(1)}, u32[]{:S(2)}, u32[]{:S(2)}) collective-permute-start(bf16[512,128]{1,0:T(8,128)(2,1)S(1)} %get-tuple-element.58), channel_id=1, source_target_pairs={{0,4},{4,8},{8,12},{12,0},{1,5},{5,9},{9,13},{13,1},{2,6},{6,10},{... | collective-permute-start | bytes 393224 | tf_op jit(solution)/shard_map/ppermute | solution.py:25
  6.0 8.0 %collective-permute-start.16 = (bf16[512,128]{1,0:T(8,128)(2,1)S(1)}, bf16[512,128]{1,0:T(8,128)(2,1)S(1)}, u32[]{:S(2)}, u32[]{:S(2)}) collective-permute-start(bf16[512,128]{1,0:T(8,128)(2,1)S(1)} %get-tuple-element.58), channel_id=1, source_target_pairs={{0,12},{4,0},{8,4},{12,8},{1,13},{5,1},{9,5},{13,9},{2,14},{6,2},{... | collective-permute-start | bytes 393224 | tf_op jit(solution)/shard_map/ppermute | solution.py:25
  8.2 8.1 %collective-permute-start.17 = (bf16[512,128]{1,0:T(8,128)(2,1)S(1)}, bf16[512,128]{1,0:T(8,128)(2,1)S(1)}, u32[]{:S(2)}, u32[]{:S(2)}) collective-permute-start(bf16[512,128]{1,0:T(8,128)(2,1)S(1)} %get-tuple-element.58), channel_id=1, source_target_pairs={{0,8},{4,12},{8,0},{12,4},{1,9},{5,13},{9,1},{13,5},{2,10},{6,14},... | collective-permute-start | bytes 393224 | tf_op jit(solution)/shard_map/ppermute | solution.py:25
  10.0 17.2 %collective-permute-start.4 = (bf16[1184,128]{1,0:T(8,128)(2,1)S(1)}, bf16[1184,128]{1,0:T(8,128)(2,1)S(1)}, u32[]{:S(2)}, u32[]{:S(2)}) collective-permute-start(bf16[1184,128]{1,0:T(8,128)(2,1)S(1)} %get-tuple-element.43), channel_id=1, source_target_pairs={{0,4},{4,8},{8,12},{12,0},{1,5},{5,9},{9,13},{13,1},{2,6},{6,10},{... | collective-permute-start | bytes 909320 | tf_op jit(solution)/shard_map/ppermute | solution.py:25
  11.3 18.1 %collective-permute-start.5 = (bf16[1184,128]{1,0:T(8,128)(2,1)S(1)}, bf16[1184,128]{1,0:T(8,128)(2,1)S(1)}, u32[]{:S(2)}, u32[]{:S(2)}) collective-permute-start(bf16[1184,128]{1,0:T(8,128)(2,1)S(1)} %get-tuple-element.43), channel_id=1, source_target_pairs={{0,12},{4,0},{8,4},{12,8},{1,13},{5,1},{9,5},{13,9},{2,14},{6,2},{... | collective-permute-start | bytes 909320 | tf_op jit(solution)/shard_map/ppermute | solution.py:25
  14.0 9.4 %collective-permute-start.1 = (bf16[4,16,2048]{2,1,0:T(8,128)(2,1)}, bf16[4,16,2048]{2,1,0:T(8,128)(2,1)S(1)}, u32[]{:S(2)}, u32[]{:S(2)}) collective-permute-start(bf16[4,16,2048]{2,1,0:T(8,128)(2,1)} %tokens.1), channel_id=1, source_target_pairs={{0,3},{1,0},{2,1},{3,2},{4,7},{5,4},{6,5},{7,6},{8,11},{9,8},{10,9... | collective-permute-start | bytes 786440 | tf_op jit(solution)/shard_map/ppermute | solution.py:25
  16.3 8.6 %collective-permute-start.2 = (bf16[4,16,2048]{2,1,0:T(8,128)(2,1)}, bf16[4,16,2048]{2,1,0:T(8,128)(2,1)S(1)}, u32[]{:S(2)}, u32[]{:S(2)}) collective-permute-start(bf16[4,16,2048]{2,1,0:T(8,128)(2,1)} %tokens.1), channel_id=1, source_target_pairs={{0,2},{1,3},{2,0},{3,1},{4,6},{5,7},{6,4},{7,5},{8,10},{9,11},{10,... | collective-permute-start | bytes 786440 | tf_op jit(solution)/shard_map/ppermute | solution.py:25
  19.2 13.5 %collective-permute-start.6 = (bf16[1184,128]{1,0:T(8,128)(2,1)S(1)}, bf16[1184,128]{1,0:T(8,128)(2,1)S(1)}, u32[]{:S(2)}, u32[]{:S(2)}) collective-permute-start(bf16[1184,128]{1,0:T(8,128)(2,1)S(1)} %get-tuple-element.43), channel_id=1, source_target_pairs={{0,8},{4,12},{8,0},{12,4},{1,9},{5,13},{9,1},{13,5},{2,10},{6,14},... | collective-permute-start | bytes 909320 | tf_op jit(solution)/shard_map/ppermute | solution.py:25
  23.4 13.3 %collective-permute-start.18 = (bf16[1536,128]{1,0:T(8,128)(2,1)S(1)}, bf16[1536,128]{1,0:T(8,128)(2,1)S(1)}, u32[]{:S(2)}, u32[]{:S(2)}) collective-permute-start(bf16[1536,128]{1,0:T(8,128)(2,1)S(1)} %shard_map.126.g0), channel_id=1, source_target_pairs={{0,32},{32,64},{64,96},{96,0},{1,33},{33,65},{65,97},{97,1},{2,34}... | collective-permute-start | bytes 1179656 | tf_op jit(solution)/shard_map/ppermute | solution.py:25
  24.9 16.6 %collective-permute-start.19 = (bf16[1536,128]{1,0:T(8,128)(2,1)S(1)}, bf16[1536,128]{1,0:T(8,128)(2,1)S(1)}, u32[]{:S(2)}, u32[]{:S(2)}) collective-permute-start(bf16[1536,128]{1,0:T(8,128)(2,1)S(1)} %shard_map.126.g0), channel_id=1, source_target_pairs={{0,96},{32,0},{64,32},{96,64},{1,97},{33,1},{65,33},{97,65},{2,98}... | collective-permute-start | bytes 1179656 | tf_op jit(solution)/shard_map/ppermute | solution.py:25
  27.2 14.4 %collective-permute-start.20 = (bf16[1536,128]{1,0:T(8,128)(2,1)S(1)}, bf16[1536,128]{1,0:T(8,128)(2,1)S(1)}, u32[]{:S(2)}, u32[]{:S(2)}) collective-permute-start(bf16[1536,128]{1,0:T(8,128)(2,1)S(1)} %shard_map.126.g0), channel_id=1, source_target_pairs={{0,64},{32,96},{64,0},{96,32},{1,65},{33,97},{65,1},{97,33},{2,66}... | collective-permute-start | bytes 1179656 | tf_op jit(solution)/shard_map/ppermute | solution.py:25
  29.4 5.2 %collective-permute-start.3 = (bf16[2,16,1024]{2,1,0:T(8,128)(2,1)S(1)}, bf16[2,16,1024]{2,1,0:T(8,128)(2,1)S(1)}, u32[]{:S(2)}, u32[]{:S(2)}) collective-permute-start(bf16[2,16,1024]{2,1,0:T(8,128)(2,1)S(1)} %get-tuple-element.38), channel_id=1, source_target_pairs={{0,4},{4,8},{8,12},{12,16},{16,20},{20,24},{24,28},{28,32},{32,36}... | collective-permute-start | bytes 196616 | tf_op jit(solution)/shard_map/ppermute | solution.py:342
  32.7 9.3 %collective-permute-start.7 = (bf16[1184,128]{1,0:T(8,128)(2,1)S(1)}, bf16[1184,128]{1,0:T(8,128)(2,1)S(1)}, u32[]{:S(2)}, u32[]{:S(2)}) collective-permute-start(bf16[1184,128]{1,0:T(8,128)(2,1)S(1)} %collective-permute-done.4.a1), channel_id=1, source_target_pairs={{0,16},{16,0},{1,17},{17,1},{2,18},{18,2},{3,19},{19,3},{4,20},{20... | collective-permute-start | bytes 909320 | tf_op jit(solution)/shard_map/ppermute | solution.py:25
  34.6 7.5 %collective-permute-start.8 = (bf16[1184,128]{1,0:T(8,128)(2,1)S(1)}, bf16[1184,128]{1,0:T(8,128)(2,1)S(1)}, u32[]{:S(2)}, u32[]{:S(2)}) collective-permute-start(bf16[1184,128]{1,0:T(8,128)(2,1)S(1)} %collective-permute-done.5.a2), channel_id=1, source_target_pairs={{0,16},{16,0},{1,17},{17,1},{2,18},{18,2},{3,19},{19,3},{4,20},{20... | collective-permute-start | bytes 909320 | tf_op jit(solution)/shard_map/ppermute | solution.py:25
  36.7 32.4 %collective-permute-start.21 = (bf16[1536,128]{1,0:T(8,128)(2,1)S(1)}, bf16[1536,128]{1,0:T(8,128)(2,1)S(1)}, u32[]{:S(2)}, u32[]{:S(2)}) collective-permute-start(bf16[1536,128]{1,0:T(8,128)(2,1)S(1)} %shard_map.126.g0), channel_id=1, source_target_pairs={{0,16},{16,0},{1,17},{17,1},{2,18},{18,2},{3,19},{19,3},{4,20},{20... | collective-permute-start | bytes 1179656 | tf_op jit(solution)/shard_map/ppermute | solution.py:25
  41.5 27.6 %collective-permute-start.22 = (bf16[1536,128]{1,0:T(8,128)(2,1)S(1)}, bf16[1536,128]{1,0:T(8,128)(2,1)S(1)}, u32[]{:S(2)}, u32[]{:S(2)}) collective-permute-start(bf16[1536,128]{1,0:T(8,128)(2,1)S(1)} %collective-permute-done.18.g1), channel_id=1, source_target_pairs={{0,16},{16,0},{1,17},{17,1},{2,18},{18,2},{3,19},{19,3},{4,20},{20... | collective-permute-start | bytes 1179656 | tf_op jit(solution)/shard_map/ppermute | solution.py:25
  41.5 27.6 %collective-permute-start.23 = (bf16[1536,128]{1,0:T(8,128)(2,1)S(1)}, bf16[1536,128]{1,0:T(8,128)(2,1)S(1)}, u32[]{:S(2)}, u32[]{:S(2)}) collective-permute-start(bf16[1536,128]{1,0:T(8,128)(2,1)S(1)} %collective-permute-done.19.g2), channel_id=1, source_target_pairs={{0,16},{16,0},{1,17},{17,1},{2,18},{18,2},{3,19},{19,3},{4,20},{20... | collective-permute-start | bytes 1179656 | tf_op jit(solution)/shard_map/ppermute | solution.py:25
  42.0 27.1 %collective-permute-start.24 = (bf16[1536,128]{1,0:T(8,128)(2,1)S(1)}, bf16[1536,128]{1,0:T(8,128)(2,1)S(1)}, u32[]{:S(2)}, u32[]{:S(2)}) collective-permute-start(bf16[1536,128]{1,0:T(8,128)(2,1)S(1)} %collective-permute-done.20.g3), channel_id=1, source_target_pairs={{0,16},{16,0},{1,17},{17,1},{2,18},{18,2},{3,19},{19,3},{4,20},{20... | collective-permute-start | bytes 1179656 | tf_op jit(solution)/shard_map/ppermute | solution.py:25
  42.1 2.7 %collective-permute-start.9 = (bf16[1184,128]{1,0:T(8,128)(2,1)S(1)}, bf16[1184,128]{1,0:T(8,128)(2,1)S(1)}, u32[]{:S(2)}, u32[]{:S(2)}) collective-permute-start(bf16[1184,128]{1,0:T(8,128)(2,1)S(1)} %collective-permute-done.6.a3), channel_id=1, source_target_pairs={{0,16},{16,0},{1,17},{17,1},{2,18},{18,2},{3,19},{19,3},{4,20},{20... | collective-permute-start | bytes 909320 | tf_op jit(solution)/shard_map/ppermute | solution.py:25
  46.9 3.8 %collective-permute-start.10 = (f32[2,4,4,128]{3,2,1,0:T(4,128)S(1)}, f32[2,4,4,128]{3,2,1,0:T(4,128)S(1)}, u32[]{:S(2)}, u32[]{:S(2)}) collective-permute-start(f32[2,4,4,128]{3,2,1,0:T(4,128)S(1)} %get-tuple-element.47.total), channel_id=1, source_target_pairs={{0,4},{4,0},{8,12},{12,8},{1,5},{5,1},{9,13},{13,9},{2,6},{6,2},{1... | collective-permute-start | bytes 49160 | tf_op jit(solution)/shard_map/ppermute | solution.py:273
  51.2 5.0 %collective-permute-start.11 = (f32[2,4,4,128]{3,2,1,0:T(4,128)S(1)}, f32[2,4,4,128]{3,2,1,0:T(4,128)S(1)}, u32[]{:S(2)}, u32[]{:S(2)}) collective-permute-start(f32[2,4,4,128]{3,2,1,0:T(4,128)S(1)} %get-tuple-element.48.total), channel_id=1, source_target_pairs={{0,12},{4,8},{8,4},{12,0},{1,13},{5,9},{9,5},{13,1},{2,14},{6,10},... | collective-permute-start | bytes 49160 | tf_op jit(solution)/shard_map/ppermute | solution.py:273
  56.8 1.3 %collective-permute-start.12 = (f32[2,4,4,128]{3,2,1,0:T(4,128)S(1)}, f32[2,4,4,128]{3,2,1,0:T(4,128)S(1)}, u32[]{:S(2)}, u32[]{:S(2)}) collective-permute-start(f32[2,4,4,128]{3,2,1,0:T(4,128)S(1)} %get-tuple-element.50.total), channel_id=1, source_target_pairs={{0,16},{16,0},{1,17},{17,1},{2,18},{18,2},{3,19},{19,3},{4,20},{20... | collective-permute-start | bytes 49160 | tf_op jit(solution)/shard_map/ppermute | solution.py:273
  58.7 3.8 %collective-permute-start.13 = (f32[2,4,4,128]{3,2,1,0:T(4,128)S(1)}, f32[2,4,4,128]{3,2,1,0:T(4,128)S(1)}, u32[]{:S(2)}, u32[]{:S(2)}) collective-permute-start(f32[2,4,4,128]{3,2,1,0:T(4,128)S(1)} %get-tuple-element.52.total), channel_id=1, source_target_pairs={{0,32},{32,0},{64,96},{96,64},{1,33},{33,1},{65,97},{97,65},{2,34}... | collective-permute-start | bytes 49160 | tf_op jit(solution)/shard_map/ppermute | solution.py:273
  63.0 5.5 %collective-permute-start.14 = (f32[2,4,4,128]{3,2,1,0:T(4,128)S(1)}, f32[2,4,4,128]{3,2,1,0:T(4,128)S(1)}, u32[]{:S(2)}, u32[]{:S(2)}) collective-permute-start(f32[2,4,4,128]{3,2,1,0:T(4,128)S(1)} %get-tuple-element.54.total), channel_id=1, source_target_pairs={{0,96},{32,64},{64,32},{96,0},{1,97},{33,65},{65,33},{97,1},{2,98}... | collective-permute-start | bytes 49160 | tf_op jit(solution)/shard_map/ppermute | solution.py:273
  72.6 11.1 %collective-permute-start.25 = (bf16[4,16,2048]{2,1,0:T(8,128)(2,1)S(1)}, bf16[4,16,2048]{2,1,0:T(8,128)(2,1)S(1)}, u32[]{:S(2)}, u32[]{:S(2)}) collective-permute-start(bf16[4,16,2048]{2,1,0:T(8,128)(2,1)S(1)} %get-tuple-element.62), channel_id=1, source_target_pairs={{0,1},{1,2},{2,3},{3,0},{4,5},{5,6},{6,7},{7,4},{8,9},{9,10},{10,1... | collective-permute-start | bytes 786440 | tf_op jit(solution)/shard_map/ppermute | solution.py:25
  77.0 8.9 %collective-permute-start.26 = (bf16[4,16,2048]{2,1,0:T(8,128)(2,1)S(1)}, bf16[4,16,2048]{2,1,0:T(8,128)(2,1)S(1)}, u32[]{:S(2)}, u32[]{:S(2)}) collective-permute-start(bf16[4,16,2048]{2,1,0:T(8,128)(2,1)S(1)} %get-tuple-element.63), channel_id=1, source_target_pairs={{0,3},{1,0},{2,1},{3,2},{4,7},{5,4},{6,5},{7,6},{8,11},{9,8},{10,9... | collective-permute-start | bytes 786440 | tf_op jit(solution)/shard_map/ppermute | solution.py:25
  77.2 11.3 %collective-permute-start.27 = (bf16[4,16,2048]{2,1,0:T(8,128)(2,1)S(1)}, bf16[4,16,2048]{2,1,0:T(8,128)(2,1)S(1)}, u32[]{:S(2)}, u32[]{:S(2)}) collective-permute-start(bf16[4,16,2048]{2,1,0:T(8,128)(2,1)S(1)} %get-tuple-element.64), channel_id=1, source_target_pairs={{0,2},{1,3},{2,0},{3,1},{4,6},{5,7},{6,4},{7,5},{8,10},{9,11},{10,... | collective-permute-start | bytes 786440 | tf_op jit(solution)/shard_map/ppermute | solution.py:25
where the time goes:
time: 90.1 us; the launch traced here: 89.9 us
  starting transfers between devices  42.6 us (47%)
  waiting for transfers between devices  33.7 us (37%)
  Pallas kernels  13.4 us (15%)
    ppermute x22, starting transfers between devices, shift(): lax.ppermute(value, axis, [(i, (i + by) % size) for i in range(size)])  32.4 us
    ppermute x22, waiting for transfers between devices, shift(): lax.ppermute(value, axis, [(i, (i + by) % size) for i in range(size)])  19.4 us
    pallas_call x12, Pallas kernels, call(): pl.pallas_call(kernel, out_shape=[hold(s, d) for s, d in outs], in_specs=...  13.4 us
    ppermute x5, waiting for transfers between devices, enter(): other = lax.ppermute(total, axis, partner)  12.5 us
    ppermute x5, starting transfers between devices, enter(): other = lax.ppermute(total, axis, partner)  6.92 us
    ppermute x1, starting transfers between devices, per_device(): lax.ppermute(halo, ('x', 'c', 'z'), [(i, i + 1) for i in range(stretches...  3.27 us
  transfers between devices with their start and end apart: 28, of which 14 were waited for; matrix products, arithmetic and copies ran while one was open for 0% of the time, Pallas kernels for 10%

commit v1 on v0

--- a/solution.py
+++ b/solution.py
@@ -37,16 +37,17 @@
     vmem = pl.BlockSpec(memory_space=pltpu.VMEM)
     anywhere = pl.BlockSpec(memory_space=pltpu.HBM)
     hold = jax.ShapeDtypeStruct if to_hbm else pltpu.VMEM
+    place = () if idx is None else (idx,)
     return pl.pallas_call(
         kernel,
         out_shape=[hold(s, d) for s, d in outs],
-        in_specs=[pl.BlockSpec(memory_space=pltpu.SMEM)]
+        in_specs=[pl.BlockSpec(memory_space=pltpu.SMEM)] * len(place)
         + [anywhere if k < far else vmem for k in range(len(ins))],
         out_specs=[vmem] * len(outs),
         scratch_shapes=list(scratch),
         compiler_params=pltpu.CompilerParams(vmem_limit_bytes=16 << 20),
     )(
-        idx,
+        *place,
         *[
             pltpu.with_memory_space_constraint(a, pltpu.HBM if k < far else pltpu.VMEM)
             for k, a in enumerate(ins)
@@ -56,7 +57,7 @@
 
 def fetch_kernel(
     idx, entry, valve, ow, tokens, gain, taps, bias, rw, rb, ew, eb, rate,
-    out_e, out_q, entry_v, valve_v, ow_v, tokens_v, gain_v, rows_v, rw_v, ew_v,
+    out_e, out_q, entry_v, valve_v, ow_v, tokens_v, gain_v, rows_v, rw_v, ew_v, flags,
     taps_v, bias_v, rb_v, eb_v, rate_v, sems,
 ):
     x, c = idx[0], idx[1]
@@ -71,6 +72,13 @@
         copy.start()
     for copy in copies:
         copy.wait()
+    flag = lax.broadcasted_iota(jnp.int32, (8, 128), 0)
+    x_at, c_at, z_at = idx[0], idx[1], idx[2]
+    signs = (z_at % 2, z_at // 2, c_at, x_at % 2, x_at // 2)
+    value = jnp.zeros((8, 128), jnp.int32)
+    for k, sign in enumerate(signs):
+        value = jnp.where(flag == k, sign, value)
+    flags[...] = value.astype(F32)
     out_e[0:HALF] = entry_v[pl.ds(pl.multiple_of(c * HALF, HALF), HALF), :]
     out_e[HALF : HALF + 128] = jnp.where(c == 0, rw_v[0], ew_v[0])
     rows = jnp.concatenate([taps_v[...], bias_v[...], rb_v[...], eb_v[...], rate_v[...]], axis=0)
@@ -88,7 +96,7 @@
         out_q[256 + n * 16 : 272 + n * 16] = rows[:, n * 128 : n * 128 + 128]
 
 
-def join_kernel(idx, q1, q2, q3, out):
+def join_kernel(q1, q2, q3, out):
     for k, q in enumerate((q1, q2, q3)):
         out[k * 512 : k * 512 + 512] = q[...]
 
@@ -234,7 +242,7 @@
         out[...] = mixed[k * 64 : k * 64 + 64].reshape(4, 16, 2048).astype(BF16)
 
 
-def mix_kernel(idx, own, r1, r2, r3, out):
+def mix_kernel(own, r1, r2, r3, out):
     total = own[...] + r1[...].astype(F32) + r2[...].astype(F32) + r3[...].astype(F32)
     out[...] = total.astype(BF16)
 
@@ -243,11 +251,10 @@
     return earlier[0] * later[0], later[0] * earlier[1] + later[1]
 
 
-def level_kernel(idx, total, other, *rest, position, mirrored, first, last):
+def level_kernel(flags, total, other, *rest, level, first, last):
     state = None if first else rest[0]
     out = rest if first else rest[1:]
-    place = idx[position]
-    upper = (place >= 2) if mirrored else (place % 2 == 1)
+    upper = jnp.broadcast_to(flags[level : level + 1, :].reshape(1, 1, 128), (4, 4, 128)) > 0.5
     mine = (total[0], total[1])
     theirs = (other[0], other[1])
     if first:
@@ -264,7 +271,7 @@
     out[1][0], out[1][1] = after(earlier, later)
 
 
-def enter(total, idx):
+def enter(total, flags):
     levels = (("z", False), ("z", True), ("c", False), ("x", False), ("x", True))
     state = None
     for k, (axis, mirrored) in enumerate(levels):
@@ -274,15 +281,14 @@
         first, last = k == 0, k == len(levels) - 1
         kernel = functools.partial(
             level_kernel,
-            position=SP_TP.index(axis),
-            mirrored=mirrored,
+            level=k,
             first=first,
             last=last,
         )
         pair = ((2, 4, 4, 128), F32)
         outs = [((4, 4, 128), F32)] if last else [pair, pair]
-        ins = (total, other) if first else (total, other, state)
-        state, *left = call(kernel, idx, ins, outs)
+        ins = (flags, total, other) if first else (flags, total, other, state)
+        state, *left = call(kernel, None, ins, outs)
         total = left[0] if left else None
     return state
 
@@ -314,14 +320,14 @@
     )
     pieces = spread(tokens, "y")
     gate = ((1, 128, 128), BF16)
-    message, eighths, entry, valve, ow, own_tokens, gain, rows, rw, ew = call(
+    message, eighths, entry, valve, ow, own_tokens, gain, rows, rw, ew, flags = call(
         fetch_kernel,
         idx,
         (entry_projection, valve_projection, output_weight, tokens, vector(norm_gain), *small),
         [
             ((HALF + 160, 128), BF16), ((512, 128), BF16), ((2048, 128), BF16),
             ((2048, 128), BF16), ((128, 2048), BF16), ((4, 16, 2048), BF16), ((1, 2048), F32),
-            ((8, 128), F32), gate, gate,
+            ((8, 128), F32), gate, gate, ((8, 128), F32),
         ],
         scratch=[pltpu.VMEM((4, 128), F32)]
         + [pltpu.VMEM((1, 128), F32)] * 4
@@ -330,7 +336,7 @@
     )
     quarters = spread(eighths, "z")
     entry_near = spread(message, "z")
-    (joined,) = call(join_kernel, idx, quarters, [((1536, 128), BF16)])
+    (joined,) = call(join_kernel, None, quarters, [((1536, 128), BF16)])
     gathered = [joined] + spread(joined, "x")
     xn, halo = call(
         norm_kernel,
@@ -349,7 +355,7 @@
         [((4, 256, 128), F32), ((4, 256, 128), F32), ((2, 4, 8, 128), F32), ((2, 4, 4, 128), F32)],
         scratch=[pltpu.VMEM((4, 280, 128), F32)],
     )
-    entering = enter(total, idx)
+    entering = enter(total, flags)
     silu, wo = call(
         prepare_kernel,
         idx,
@@ -365,7 +371,7 @@
         scratch=[pltpu.VMEM((4, 256, 128), F32), pltpu.VMEM((4, 64, 512), BF16)],
     )
     parts = [shift(p, "y", by) for p, by in zip(parts, SHIFTS)]
-    (mixed,) = call(mix_kernel, idx, (own, *parts), [((4, 16, 2048), BF16)], to_hbm=True)
+    (mixed,) = call(mix_kernel, None, (own, *parts), [((4, 16, 2048), BF16)], to_hbm=True)
     return mixed
 
 

time: 90.1 us -> 86.8 us (0.963)
  Pallas kernels: 13.4 us -> 9.61 us
    pallas_call x12, Pallas kernels: 13.4 us -> 9.61 us  [call(): pl.pallas_call(kernel, out_shape=[hold(s, d) for s, d in outs], in_specs=...]
  transfers between devices with their start and end apart: 28 -> 28, of which waited for: 14 -> 14; matrix products, arithmetic and copies ran while one was open for 0% -> 0% of each run, Pallas kernels for 10% -> 6%
where the time goes in v1:
time: 86.8 us; the launch traced here: 86.6 us
  starting transfers between devices  42.6 us (49%)
  waiting for transfers between devices  34.2 us (39%)
  Pallas kernels  9.61 us (11%)
    ppermute x22, starting transfers between devices, shift(): lax.ppermute(value, axis, [(i, (i + by) % size) for i in range(size)])  32.4 us
    ppermute x22, waiting for transfers between devices, shift(): lax.ppermute(value, axis, [(i, (i + by) % size) for i in range(size)])  20 us
    ppermute x5, waiting for transfers between devices, enter(): other = lax.ppermute(total, axis, partner)  12.5 us
    pallas_call x12, Pallas kernels, call(): pl.pallas_call(kernel, out_shape=[hold(s, d) for s, d in outs], in_specs=...  9.61 us
    ppermute x5, starting transfers between devices, enter(): other = lax.ppermute(total, axis, partner)  6.91 us
    ppermute x1, starting transfers between devices, per_device(): lax.ppermute(halo, ('x', 'c', 'z'), [(i, i + 1) for i in range(stretches...  3.27 us
    ppermute x1, waiting for transfers between devices, per_device(): lax.ppermute(halo, ('x', 'c', 'z'), [(i, i + 1) for i in range(stretches...  1.78 us
  transfers between devices with their start and end apart: 28, of which 14 were waited for; matrix products, arithmetic and copies ran while one was open for 0% of the time, Pallas kernels for 6%

profile of v1, /device:TPU:0, one launch (start us, length us, event | category | flops | bytes accessed | tf_op | source)
XLA Modules:
  0.0 86.6 jit_solution(4591056362841888180)
XLA Ops:
  0.0 1.7 %collective-permute-start = (bf16[4,16,2048]{2,1,0:T(8,128)(2,1)}, bf16[4,16,2048]{2,1,0:T(8,128)(2,1)S(1)}, u32[]{:S(2)}, u32[]{:S(2)}) collective-permute-start(bf16[4,16,2048]{2,1,0:T(8,128)(2,1)} %tokens.1), channel_id=1, source_target_pairs={{0,1},{1,2},{2,3},{3,0},{4,5},{5,6},{6,7},{7,4},{8,9},{9,10},{10,1... | collective-permute-start | bytes 786440 | tf_op jit(solution)/shard_map/ppermute | solution.py:25
  1.7 0.1 pad_add_fusion.idx
  1.8 2.2 %shard_map.118 = (bf16[1184,128]{1,0:T(8,128)(2,1)S(1)}, bf16[512,128]{1,0:T(8,128)(2,1)S(1)}, bf16[2048,128]{1,0:T(8,128)(2,1)S(1)}, bf16[2048,128]{1,0:T(8,128...) custom-call(s32[4]{0:T(128)S(1)} %pad_add_fusion.idx, ...), custom_call_target="tpu_custom_call" | custom-call | tf_op jit(solution)/shard_map/pallas_call | solution.py:41
  4.0 2.0 %collective-permute-start.15 = (bf16[512,128]{1,0:T(8,128)(2,1)S(1)}, bf16[512,128]{1,0:T(8,128)(2,1)S(1)}, u32[]{:S(2)}, u32[]{:S(2)}) collective-permute-start(bf16[512,128]{1,0:T(8,128)(2,1)S(1)} %get-tuple-element.60), channel_id=1, source_target_pairs={{0,4},{4,8},{8,12},{12,0},{1,5},{5,9},{9,13},{13,1},{2,6},{6,10},{... | collective-permute-start | bytes 393224 | tf_op jit(solution)/shard_map/ppermute | solution.py:25
  6.0 2.2 %collective-permute-start.16 = (bf16[512,128]{1,0:T(8,128)(2,1)S(1)}, bf16[512,128]{1,0:T(8,128)(2,1)S(1)}, u32[]{:S(2)}, u32[]{:S(2)}) collective-permute-start(bf16[512,128]{1,0:T(8,128)(2,1)S(1)} %get-tuple-element.60), channel_id=1, source_target_pairs={{0,12},{4,0},{8,4},{12,8},{1,13},{5,1},{9,5},{13,9},{2,14},{6,2},{... | collective-permute-start | bytes 393224 | tf_op jit(solution)/shard_map/ppermute | solution.py:25
  8.2 1.8 %collective-permute-start.17 = (bf16[512,128]{1,0:T(8,128)(2,1)S(1)}, bf16[512,128]{1,0:T(8,128)(2,1)S(1)}, u32[]{:S(2)}, u32[]{:S(2)}) collective-permute-start(bf16[512,128]{1,0:T(8,128)(2,1)S(1)} %get-tuple-element.60), channel_id=1, source_target_pairs={{0,8},{4,12},{8,0},{12,4},{1,9},{5,13},{9,1},{13,5},{2,10},{6,14},... | collective-permute-start | bytes 393224 | tf_op jit(solution)/shard_map/ppermute | solution.py:25
  10.0 1.0 %collective-permute-start.4 = (bf16[1184,128]{1,0:T(8,128)(2,1)S(1)}, bf16[1184,128]{1,0:T(8,128)(2,1)S(1)}, u32[]{:S(2)}, u32[]{:S(2)}) collective-permute-start(bf16[1184,128]{1,0:T(8,128)(2,1)S(1)} %get-tuple-element.44), channel_id=1, source_target_pairs={{0,4},{4,8},{8,12},{12,0},{1,5},{5,9},{9,13},{13,1},{2,6},{6,10},{... | collective-permute-start | bytes 909320 | tf_op jit(solution)/shard_map/ppermute | solution.py:25
  11.0 0.3 collective-permute-done.15.q1
  11.3 2.7 %collective-permute-start.5 = (bf16[1184,128]{1,0:T(8,128)(2,1)S(1)}, bf16[1184,128]{1,0:T(8,128)(2,1)S(1)}, u32[]{:S(2)}, u32[]{:S(2)}) collective-permute-start(bf16[1184,128]{1,0:T(8,128)(2,1)S(1)} %get-tuple-element.44), channel_id=1, source_target_pairs={{0,12},{4,0},{8,4},{12,8},{1,13},{5,1},{9,5},{13,9},{2,14},{6,2},{... | collective-permute-start | bytes 909320 | tf_op jit(solution)/shard_map/ppermute | solution.py:25
  14.0 1.7 %collective-permute-start.1 = (bf16[4,16,2048]{2,1,0:T(8,128)(2,1)}, bf16[4,16,2048]{2,1,0:T(8,128)(2,1)S(1)}, u32[]{:S(2)}, u32[]{:S(2)}) collective-permute-start(bf16[4,16,2048]{2,1,0:T(8,128)(2,1)} %tokens.1), channel_id=1, source_target_pairs={{0,3},{1,0},{2,1},{3,2},{4,7},{5,4},{6,5},{7,6},{8,11},{9,8},{10,9... | collective-permute-start | bytes 786440 | tf_op jit(solution)/shard_map/ppermute | solution.py:25
  15.7 0.5 collective-permute-done.17.q3
  16.3 2.9 %collective-permute-start.2 = (bf16[4,16,2048]{2,1,0:T(8,128)(2,1)}, bf16[4,16,2048]{2,1,0:T(8,128)(2,1)S(1)}, u32[]{:S(2)}, u32[]{:S(2)}) collective-permute-start(bf16[4,16,2048]{2,1,0:T(8,128)(2,1)} %tokens.1), channel_id=1, source_target_pairs={{0,2},{1,3},{2,0},{3,1},{4,6},{5,7},{6,4},{7,5},{8,10},{9,11},{10,... | collective-permute-start | bytes 786440 | tf_op jit(solution)/shard_map/ppermute | solution.py:25
  19.2 1.6 %collective-permute-start.6 = (bf16[1184,128]{1,0:T(8,128)(2,1)S(1)}, bf16[1184,128]{1,0:T(8,128)(2,1)S(1)}, u32[]{:S(2)}, u32[]{:S(2)}) collective-permute-start(bf16[1184,128]{1,0:T(8,128)(2,1)S(1)} %get-tuple-element.44), channel_id=1, source_target_pairs={{0,8},{4,12},{8,0},{12,4},{1,9},{5,13},{9,1},{13,5},{2,10},{6,14},... | collective-permute-start | bytes 909320 | tf_op jit(solution)/shard_map/ppermute | solution.py:25
  20.8 2.6 %collective-permute-done.1.t2 = bf16[4,16,2048]{2,1,0:T(8,128)(2,1)S(1)} collective-permute-done((bf16[4,16,2048]{2,1,0:T(8,128)(2,1)}, bf16[4,16,2048]{2,1,0:T(8,128)(2,1)S(1)}, u32[]{:S(2)}, u32[]{:S(2)}) %collective-permute-start.1) | collective-permute-done | bytes 262176 | tf_op jit(solution)/shard_map/ppermute | solution.py:25
  23.4 1.5 %collective-permute-start.18 = (bf16[1536,128]{1,0:T(8,128)(2,1)S(1)}, bf16[1536,128]{1,0:T(8,128)(2,1)S(1)}, u32[]{:S(2)}, u32[]{:S(2)}) collective-permute-start(bf16[1536,128]{1,0:T(8,128)(2,1)S(1)} %shard_map.126.g0), channel_id=1, source_target_pairs={{0,32},{32,64},{64,96},{96,0},{1,33},{33,65},{65,97},{97,1},{2,34}... | collective-permute-start | bytes 1179656 | tf_op jit(solution)/shard_map/ppermute | solution.py:25
  24.9 2.3 %collective-permute-start.19 = (bf16[1536,128]{1,0:T(8,128)(2,1)S(1)}, bf16[1536,128]{1,0:T(8,128)(2,1)S(1)}, u32[]{:S(2)}, u32[]{:S(2)}) collective-permute-start(bf16[1536,128]{1,0:T(8,128)(2,1)S(1)} %shard_map.126.g0), channel_id=1, source_target_pairs={{0,96},{32,0},{64,32},{96,64},{1,97},{33,1},{65,33},{97,65},{2,98}... | collective-permute-start | bytes 1179656 | tf_op jit(solution)/shard_map/ppermute | solution.py:25
  27.2 1.3 %collective-permute-start.20 = (bf16[1536,128]{1,0:T(8,128)(2,1)S(1)}, bf16[1536,128]{1,0:T(8,128)(2,1)S(1)}, u32[]{:S(2)}, u32[]{:S(2)}) collective-permute-start(bf16[1536,128]{1,0:T(8,128)(2,1)S(1)} %shard_map.126.g0), channel_id=1, source_target_pairs={{0,64},{32,96},{64,0},{96,32},{1,65},{33,97},{65,1},{97,33},{2,66}... | collective-permute-start | bytes 1179656 | tf_op jit(solution)/shard_map/ppermute | solution.py:25
  28.4 1.0 %shard_map.119 = (bf16[2,4,64,1024]{3,2,1,0:T(8,128)(2,1)S(1)}, bf16[2,16,1024]{2,1,0:T(8,128)(2,1)S(1)}) custom-call(s32[4]{0:T(128)S(1)} %pad_add_fusion.idx, bf16[4,16,2048]{2,1,0:T(8,128)(2,1)S(1)} %get-tuple-element.36.t0, bf16[4,16,2048]{2,1,0:T(8,128)(2,1)S(1)} %collective-permute-done.t1, bf16[4,16,2048]{2,1,0:T(8,128)(2,1)S(1)} %collective-permute-done.1.t2, ...), custom_call_target="tpu_custom_call" | custom-call | tf_op jit(solution)/shard_map/pallas_call | solution.py:41
  29.4 3.3 %collective-permute-start.3 = (bf16[2,16,1024]{2,1,0:T(8,128)(2,1)S(1)}, bf16[2,16,1024]{2,1,0:T(8,128)(2,1)S(1)}, u32[]{:S(2)}, u32[]{:S(2)}) collective-permute-start(bf16[2,16,1024]{2,1,0:T(8,128)(2,1)S(1)} %get-tuple-element.39), channel_id=1, source_target_pairs={{0,4},{4,8},{8,12},{12,16},{16,20},{20,24},{24,28},{28,32},{32,36}... | collective-permute-start | bytes 196616 | tf_op jit(solution)/shard_map/ppermute | solution.py:348
  32.7 0.1 collective-permute-start.7
  32.8 1.8 %collective-permute-done.3.halo = bf16[2,16,1024]{2,1,0:T(8,128)(2,1)S(1)} collective-permute-done((bf16[2,16,1024]{2,1,0:T(8,128)(2,1)S(1)}, bf16[2,16,1024]{2,1,0:T(8,128)(2,1)S(1)}, u32[]{:S(2)}, u32[]{:S(2)}) %collective-permute-start.3) | collective-permute-done | bytes 65568 | tf_op jit(solution)/shard_map/ppermute | solution.py:348
  34.6 2.1 %collective-permute-start.8 = (bf16[1184,128]{1,0:T(8,128)(2,1)S(1)}, bf16[1184,128]{1,0:T(8,128)(2,1)S(1)}, u32[]{:S(2)}, u32[]{:S(2)}) collective-permute-start(bf16[1184,128]{1,0:T(8,128)(2,1)S(1)} %collective-permute-done.5.a2), channel_id=1, source_target_pairs={{0,16},{16,0},{1,17},{17,1},{2,18},{18,2},{3,19},{19,3},{4,20},{20... | collective-permute-start | bytes 909320 | tf_op jit(solution)/shard_map/ppermute | solution.py:25
  36.7 0.0 collective-permute-start.21
  36.7 4.8 %collective-permute-done.19.g2 = bf16[1536,128]{1,0:T(8,128)(2,1)S(1)} collective-permute-done((bf16[1536,128]{1,0:T(8,128)(2,1)S(1)}, bf16[1536,128]{1,0:T(8,128)(2,1)S(1)}, u32[]{:S(2)}, u32[]{:S(2)}) %collective-permute-start.19) | collective-permute-done | bytes 393248 | tf_op jit(solution)/shard_map/ppermute | solution.py:25
  41.5 0.5 collective-permute-start.23
  42.0 0.1 collective-permute-start.24
  42.1 0.4 collective-permute-start.9
  42.6 2.2 %collective-permute-done.9.b3 = bf16[1184,128]{1,0:T(8,128)(2,1)S(1)} collective-permute-done((bf16[1184,128]{1,0:T(8,128)(2,1)S(1)}, bf16[1184,128]{1,0:T(8,128)(2,1)S(1)}, u32[]{:S(2)}, u32[]{:S(2)}) %collective-permute-start.9) | collective-permute-done | bytes 303136 | tf_op jit(solution)/shard_map/ppermute | solution.py:25
  44.8 2.0 %shard_map.120 = (f32[4,256,128]{2,1,0:T(8,128)S(1)}, f32[4,256,128]{2,1,0:T(8,128)S(1)}, f32[2,4,8,128]{3,2,1,0:T(8,128)S(1)}, f32[2,4,4,128]{3,2,1,0:T(4,128)S(1)}) custom-call(s32[4]{0:T(128)S(1)} %pad_add_fusion.idx, bf16[2,4,64,1024]{3,2,1,0:T(8,128)(2,1)S(1)} %get-tuple-element.38.xn, bf16[2,16,1024]{2,1,0:T(8,128)(2,1)S(1)} %collective-permute-done.3.halo, ...), custom_call_target="tpu_custom_call" | custom-call | tf_op jit(solution)/shard_map/pallas_call | solution.py:41
  46.9 0.1 collective-permute-start.10
  47.0 3.7 %collective-permute-done.10.other = f32[2,4,4,128]{3,2,1,0:T(4,128)S(1)} collective-permute-done((f32[2,4,4,128]{3,2,1,0:T(4,128)S(1)}, f32[2,4,4,128]{3,2,1,0:T(4,128)S(1)}, u32[]{:S(2)}, u32[]{:S(2)}) %collective-permute-start.10) | collective-permute-done | bytes 16416 | tf_op jit(solution)/shard_map/ppermute | solution.py:280
  50.7 1.4 %collective-permute-start.11 = (f32[2,4,4,128]{3,2,1,0:T(4,128)S(1)}, f32[2,4,4,128]{3,2,1,0:T(4,128)S(1)}, u32[]{:S(2)}, u32[]{:S(2)}) collective-permute-start(f32[2,4,4,128]{3,2,1,0:T(4,128)S(1)} %get-tuple-element.50.total), channel_id=1, source_target_pairs={{0,12},{4,8},{8,4},{12,0},{1,13},{5,9},{9,5},{13,1},{2,14},{6,10},... | collective-permute-start | bytes 49160 | tf_op jit(solution)/shard_map/ppermute | solution.py:280
  52.1 3.6 %collective-permute-done.11.other = f32[2,4,4,128]{3,2,1,0:T(4,128)S(1)} collective-permute-done((f32[2,4,4,128]{3,2,1,0:T(4,128)S(1)}, f32[2,4,4,128]{3,2,1,0:T(4,128)S(1)}, u32[]{:S(2)}, u32[]{:S(2)}) %collective-permute-start.11) | collective-permute-done | bytes 16416 | tf_op jit(solution)/shard_map/ppermute | solution.py:280
  55.7 0.1 collective-permute-start.12
  55.8 1.2 %collective-permute-done.12.other = f32[2,4,4,128]{3,2,1,0:T(4,128)S(1)} collective-permute-done((f32[2,4,4,128]{3,2,1,0:T(4,128)S(1)}, f32[2,4,4,128]{3,2,1,0:T(4,128)S(1)}, u32[]{:S(2)}, u32[]{:S(2)}) %collective-permute-start.12) | collective-permute-done | bytes 16416 | tf_op jit(solution)/shard_map/ppermute | solution.py:280
  57.0 1.6 %collective-permute-start.13 = (f32[2,4,4,128]{3,2,1,0:T(4,128)S(1)}, f32[2,4,4,128]{3,2,1,0:T(4,128)S(1)}, u32[]{:S(2)}, u32[]{:S(2)}) collective-permute-start(f32[2,4,4,128]{3,2,1,0:T(4,128)S(1)} %get-tuple-element.54.total), channel_id=1, source_target_pairs={{0,32},{32,0},{64,96},{96,64},{1,33},{33,1},{65,97},{97,65},{2,34}... | collective-permute-start | bytes 49160 | tf_op jit(solution)/shard_map/ppermute | solution.py:280
  58.6 2.2 %collective-permute-done.13.other = f32[2,4,4,128]{3,2,1,0:T(4,128)S(1)} collective-permute-done((f32[2,4,4,128]{3,2,1,0:T(4,128)S(1)}, f32[2,4,4,128]{3,2,1,0:T(4,128)S(1)}, u32[]{:S(2)}, u32[]{:S(2)}) %collective-permute-start.13) | collective-permute-done | bytes 16416 | tf_op jit(solution)/shard_map/ppermute | solution.py:280
  60.8 3.7 %collective-permute-start.14 = (f32[2,4,4,128]{3,2,1,0:T(4,128)S(1)}, f32[2,4,4,128]{3,2,1,0:T(4,128)S(1)}, u32[]{:S(2)}, u32[]{:S(2)}) collective-permute-start(f32[2,4,4,128]{3,2,1,0:T(4,128)S(1)} %get-tuple-element.56.total), channel_id=1, source_target_pairs={{0,96},{32,64},{64,32},{96,0},{1,97},{33,65},{65,33},{97,1},{2,98}... | collective-permute-start | bytes 49160 | tf_op jit(solution)/shard_map/ppermute | solution.py:280
  64.6 1.7 %collective-permute-done.14.other = f32[2,4,4,128]{3,2,1,0:T(4,128)S(1)} collective-permute-done((f32[2,4,4,128]{3,2,1,0:T(4,128)S(1)}, f32[2,4,4,128]{3,2,1,0:T(4,128)S(1)}, u32[]{:S(2)}, u32[]{:S(2)}) %collective-permute-start.14) | collective-permute-done | bytes 16416 | tf_op jit(solution)/shard_map/ppermute | solution.py:280
  66.4 2.0 %shard_map.127 = (f32[256,512]{1,0:T(8,128)S(1)}, bf16[512,2048]{1,0:T(8,128)(2,1)S(1)}) custom-call(s32[4]{0:T(128)S(1)} %pad_add_fusion.idx, bf16[2,4,64,1024]{3,2,1,0:T(8,128)(2,1)S(1)} %get-tuple-element.38.xn, bf16[2048,128]{1,0:T(8,128)(2,1)S(1)} %get-tuple-element.58.valve, bf16[128,2048]{1,0:T(8,128)(2,1)S(1)} %get-tuple-element.59.ow, ...), custom_call_target="tpu_custom_call" | custom-call | tf_op jit(solution)/shard_map/pallas_call | solution.py:41
  68.3 1.5 %shard_map.128 = (f32[4,16,2048]{2,1,0:T(8,128)S(1)}, bf16[4,16,2048]{2,1,0:T(8,128)(2,1)S(1)}, bf16[4,16,2048]{2,1,0:T(8,128)(2,1)S(1)}, bf16[4,16,2048]{2,1,0:T(8,128)(2,1)S(1)}) custom-call(s32[4]{0:T(128)S(1)} %pad_add_fusion.idx, f32[4,256,128]{2,1,0:T(8,128)S(1)} %get-tuple-element.45.hloc, f32[4,256,128]{2,1,0:T(8,128)S(1)} %get-tuple-element.46.acum, ...), custom_call_target="tpu_custom_call" | custom-call | tf_op jit(solution)/shard_map/pallas_call | solution.py:41
  69.8 4.4 %collective-permute-start.25 = (bf16[4,16,2048]{2,1,0:T(8,128)(2,1)S(1)}, bf16[4,16,2048]{2,1,0:T(8,128)(2,1)S(1)}, u32[]{:S(2)}, u32[]{:S(2)}) collective-permute-start(bf16[4,16,2048]{2,1,0:T(8,128)(2,1)S(1)} %get-tuple-element.64), channel_id=1, source_target_pairs={{0,1},{1,2},{2,3},{3,0},{4,5},{5,6},{6,7},{7,4},{8,9},{9,10},{10,1... | collective-permute-start | bytes 786440 | tf_op jit(solution)/shard_map/ppermute | solution.py:25
  74.2 0.2 collective-permute-start.26
  74.4 1.9 %collective-permute-start.27 = (bf16[4,16,2048]{2,1,0:T(8,128)(2,1)S(1)}, bf16[4,16,2048]{2,1,0:T(8,128)(2,1)S(1)}, u32[]{:S(2)}, u32[]{:S(2)}) collective-permute-start(bf16[4,16,2048]{2,1,0:T(8,128)(2,1)S(1)} %get-tuple-element.66), channel_id=1, source_target_pairs={{0,2},{1,3},{2,0},{3,1},{4,6},{5,7},{6,4},{7,5},{8,10},{9,11},{10,... | collective-permute-start | bytes 786440 | tf_op jit(solution)/shard_map/ppermute | solution.py:25
  76.4 4.5 %collective-permute-done.25.r1 = bf16[4,16,2048]{2,1,0:T(8,128)(2,1)S(1)} collective-permute-done((bf16[4,16,2048]{2,1,0:T(8,128)(2,1)S(1)}, bf16[4,16,2048]{2,1,0:T(8,128)(2,1)S(1)}, u32[]{:S(2)}, u32[]{:S(2)}) %collective-permute-start.25) | collective-permute-done | bytes 262176 | tf_op jit(solution)/shard_map/ppermute | solution.py:25
  80.9 2.2 %collective-permute-done.26.r2 = bf16[4,16,2048]{2,1,0:T(8,128)(2,1)S(1)} collective-permute-done((bf16[4,16,2048]{2,1,0:T(8,128)(2,1)S(1)}, bf16[4,16,2048]{2,1,0:T(8,128)(2,1)S(1)}, u32[]{:S(2)}, u32[]{:S(2)}) %collective-permute-start.26) | collective-permute-done | bytes 262176 | tf_op jit(solution)/shard_map/ppermute | solution.py:25
  83.1 2.7 %collective-permute-done.27.r3 = bf16[4,16,2048]{2,1,0:T(8,128)(2,1)S(1)} collective-permute-done((bf16[4,16,2048]{2,1,0:T(8,128)(2,1)S(1)}, bf16[4,16,2048]{2,1,0:T(8,128)(2,1)S(1)}, u32[]{:S(2)}, u32[]{:S(2)}) %collective-permute-start.27) | collective-permute-done | bytes 262176 | tf_op jit(solution)/shard_map/ppermute | solution.py:25
  85.8 0.8 shard_map.129
  (21 shorter events, 0.1 us)
Async XLA Ops:
  0.0 19.2 %collective-permute-start = (bf16[4,16,2048]{2,1,0:T(8,128)(2,1)}, bf16[4,16,2048]{2,1,0:T(8,128)(2,1)S(1)}, u32[]{:S(2)}, u32[]{:S(2)}) collective-permute-start(bf16[4,16,2048]{2,1,0:T(8,128)(2,1)} %tokens.1), channel_id=1, source_target_pairs={{0,1},{1,2},{2,3},{3,0},{4,5},{5,6},{6,7},{7,4},{8,9},{9,10},{10,1... | collective-permute-start | bytes 786440 | tf_op jit(solution)/shard_map/ppermute | solution.py:25
  4.0 7.3 %collective-permute-start.15 = (bf16[512,128]{1,0:T(8,128)(2,1)S(1)}, bf16[512,128]{1,0:T(8,128)(2,1)S(1)}, u32[]{:S(2)}, u32[]{:S(2)}) collective-permute-start(bf16[512,128]{1,0:T(8,128)(2,1)S(1)} %get-tuple-element.60), channel_id=1, source_target_pairs={{0,4},{4,8},{8,12},{12,0},{1,5},{5,9},{9,13},{13,1},{2,6},{6,10},{... | collective-permute-start | bytes 393224 | tf_op jit(solution)/shard_map/ppermute | solution.py:25
  6.0 8.0 %collective-permute-start.16 = (bf16[512,128]{1,0:T(8,128)(2,1)S(1)}, bf16[512,128]{1,0:T(8,128)(2,1)S(1)}, u32[]{:S(2)}, u32[]{:S(2)}) collective-permute-start(bf16[512,128]{1,0:T(8,128)(2,1)S(1)} %get-tuple-element.60), channel_id=1, source_target_pairs={{0,12},{4,0},{8,4},{12,8},{1,13},{5,1},{9,5},{13,9},{2,14},{6,2},{... | collective-permute-start | bytes 393224 | tf_op jit(solution)/shard_map/ppermute | solution.py:25
  8.2 8.1 %collective-permute-start.17 = (bf16[512,128]{1,0:T(8,128)(2,1)S(1)}, bf16[512,128]{1,0:T(8,128)(2,1)S(1)}, u32[]{:S(2)}, u32[]{:S(2)}) collective-permute-start(bf16[512,128]{1,0:T(8,128)(2,1)S(1)} %get-tuple-element.60), channel_id=1, source_target_pairs={{0,8},{4,12},{8,0},{12,4},{1,9},{5,13},{9,1},{13,5},{2,10},{6,14},... | collective-permute-start | bytes 393224 | tf_op jit(solution)/shard_map/ppermute | solution.py:25
  10.0 17.2 %collective-permute-start.4 = (bf16[1184,128]{1,0:T(8,128)(2,1)S(1)}, bf16[1184,128]{1,0:T(8,128)(2,1)S(1)}, u32[]{:S(2)}, u32[]{:S(2)}) collective-permute-start(bf16[1184,128]{1,0:T(8,128)(2,1)S(1)} %get-tuple-element.44), channel_id=1, source_target_pairs={{0,4},{4,8},{8,12},{12,0},{1,5},{5,9},{9,13},{13,1},{2,6},{6,10},{... | collective-permute-start | bytes 909320 | tf_op jit(solution)/shard_map/ppermute | solution.py:25
  11.3 18.1 %collective-permute-start.5 = (bf16[1184,128]{1,0:T(8,128)(2,1)S(1)}, bf16[1184,128]{1,0:T(8,128)(2,1)S(1)}, u32[]{:S(2)}, u32[]{:S(2)}) collective-permute-start(bf16[1184,128]{1,0:T(8,128)(2,1)S(1)} %get-tuple-element.44), channel_id=1, source_target_pairs={{0,12},{4,0},{8,4},{12,8},{1,13},{5,1},{9,5},{13,9},{2,14},{6,2},{... | collective-permute-start | bytes 909320 | tf_op jit(solution)/shard_map/ppermute | solution.py:25
  14.0 9.4 %collective-permute-start.1 = (bf16[4,16,2048]{2,1,0:T(8,128)(2,1)}, bf16[4,16,2048]{2,1,0:T(8,128)(2,1)S(1)}, u32[]{:S(2)}, u32[]{:S(2)}) collective-permute-start(bf16[4,16,2048]{2,1,0:T(8,128)(2,1)} %tokens.1), channel_id=1, source_target_pairs={{0,3},{1,0},{2,1},{3,2},{4,7},{5,4},{6,5},{7,6},{8,11},{9,8},{10,9... | collective-permute-start | bytes 786440 | tf_op jit(solution)/shard_map/ppermute | solution.py:25
  16.3 8.6 %collective-permute-start.2 = (bf16[4,16,2048]{2,1,0:T(8,128)(2,1)}, bf16[4,16,2048]{2,1,0:T(8,128)(2,1)S(1)}, u32[]{:S(2)}, u32[]{:S(2)}) collective-permute-start(bf16[4,16,2048]{2,1,0:T(8,128)(2,1)} %tokens.1), channel_id=1, source_target_pairs={{0,2},{1,3},{2,0},{3,1},{4,6},{5,7},{6,4},{7,5},{8,10},{9,11},{10,... | collective-permute-start | bytes 786440 | tf_op jit(solution)/shard_map/ppermute | solution.py:25
  19.2 13.5 %collective-permute-start.6 = (bf16[1184,128]{1,0:T(8,128)(2,1)S(1)}, bf16[1184,128]{1,0:T(8,128)(2,1)S(1)}, u32[]{:S(2)}, u32[]{:S(2)}) collective-permute-start(bf16[1184,128]{1,0:T(8,128)(2,1)S(1)} %get-tuple-element.44), channel_id=1, source_target_pairs={{0,8},{4,12},{8,0},{12,4},{1,9},{5,13},{9,1},{13,5},{2,10},{6,14},... | collective-permute-start | bytes 909320 | tf_op jit(solution)/shard_map/ppermute | solution.py:25
  23.4 13.3 %collective-permute-start.18 = (bf16[1536,128]{1,0:T(8,128)(2,1)S(1)}, bf16[1536,128]{1,0:T(8,128)(2,1)S(1)}, u32[]{:S(2)}, u32[]{:S(2)}) collective-permute-start(bf16[1536,128]{1,0:T(8,128)(2,1)S(1)} %shard_map.126.g0), channel_id=1, source_target_pairs={{0,32},{32,64},{64,96},{96,0},{1,33},{33,65},{65,97},{97,1},{2,34}... | collective-permute-start | bytes 1179656 | tf_op jit(solution)/shard_map/ppermute | solution.py:25
  24.9 16.6 %collective-permute-start.19 = (bf16[1536,128]{1,0:T(8,128)(2,1)S(1)}, bf16[1536,128]{1,0:T(8,128)(2,1)S(1)}, u32[]{:S(2)}, u32[]{:S(2)}) collective-permute-start(bf16[1536,128]{1,0:T(8,128)(2,1)S(1)} %shard_map.126.g0), channel_id=1, source_target_pairs={{0,96},{32,0},{64,32},{96,64},{1,97},{33,1},{65,33},{97,65},{2,98}... | collective-permute-start | bytes 1179656 | tf_op jit(solution)/shard_map/ppermute | solution.py:25
  27.2 14.4 %collective-permute-start.20 = (bf16[1536,128]{1,0:T(8,128)(2,1)S(1)}, bf16[1536,128]{1,0:T(8,128)(2,1)S(1)}, u32[]{:S(2)}, u32[]{:S(2)}) collective-permute-start(bf16[1536,128]{1,0:T(8,128)(2,1)S(1)} %shard_map.126.g0), channel_id=1, source_target_pairs={{0,64},{32,96},{64,0},{96,32},{1,65},{33,97},{65,1},{97,33},{2,66}... | collective-permute-start | bytes 1179656 | tf_op jit(solution)/shard_map/ppermute | solution.py:25
  29.4 5.2 %collective-permute-start.3 = (bf16[2,16,1024]{2,1,0:T(8,128)(2,1)S(1)}, bf16[2,16,1024]{2,1,0:T(8,128)(2,1)S(1)}, u32[]{:S(2)}, u32[]{:S(2)}) collective-permute-start(bf16[2,16,1024]{2,1,0:T(8,128)(2,1)S(1)} %get-tuple-element.39), channel_id=1, source_target_pairs={{0,4},{4,8},{8,12},{12,16},{16,20},{20,24},{24,28},{28,32},{32,36}... | collective-permute-start | bytes 196616 | tf_op jit(solution)/shard_map/ppermute | solution.py:348
  32.7 9.3 %collective-permute-start.7 = (bf16[1184,128]{1,0:T(8,128)(2,1)S(1)}, bf16[1184,128]{1,0:T(8,128)(2,1)S(1)}, u32[]{:S(2)}, u32[]{:S(2)}) collective-permute-start(bf16[1184,128]{1,0:T(8,128)(2,1)S(1)} %collective-permute-done.4.a1), channel_id=1, source_target_pairs={{0,16},{16,0},{1,17},{17,1},{2,18},{18,2},{3,19},{19,3},{4,20},{20... | collective-permute-start | bytes 909320 | tf_op jit(solution)/shard_map/ppermute | solution.py:25
  34.6 7.5 %collective-permute-start.8 = (bf16[1184,128]{1,0:T(8,128)(2,1)S(1)}, bf16[1184,128]{1,0:T(8,128)(2,1)S(1)}, u32[]{:S(2)}, u32[]{:S(2)}) collective-permute-start(bf16[1184,128]{1,0:T(8,128)(2,1)S(1)} %collective-permute-done.5.a2), channel_id=1, source_target_pairs={{0,16},{16,0},{1,17},{17,1},{2,18},{18,2},{3,19},{19,3},{4,20},{20... | collective-permute-start | bytes 909320 | tf_op jit(solution)/shard_map/ppermute | solution.py:25
  36.7 29.6 %collective-permute-start.21 = (bf16[1536,128]{1,0:T(8,128)(2,1)S(1)}, bf16[1536,128]{1,0:T(8,128)(2,1)S(1)}, u32[]{:S(2)}, u32[]{:S(2)}) collective-permute-start(bf16[1536,128]{1,0:T(8,128)(2,1)S(1)} %shard_map.126.g0), channel_id=1, source_target_pairs={{0,16},{16,0},{1,17},{17,1},{2,18},{18,2},{3,19},{19,3},{4,20},{20... | collective-permute-start | bytes 1179656 | tf_op jit(solution)/shard_map/ppermute | solution.py:25
  41.5 24.8 %collective-permute-start.22 = (bf16[1536,128]{1,0:T(8,128)(2,1)S(1)}, bf16[1536,128]{1,0:T(8,128)(2,1)S(1)}, u32[]{:S(2)}, u32[]{:S(2)}) collective-permute-start(bf16[1536,128]{1,0:T(8,128)(2,1)S(1)} %collective-permute-done.18.g1), channel_id=1, source_target_pairs={{0,16},{16,0},{1,17},{17,1},{2,18},{18,2},{3,19},{19,3},{4,20},{20... | collective-permute-start | bytes 1179656 | tf_op jit(solution)/shard_map/ppermute | solution.py:25
  41.5 24.8 %collective-permute-start.23 = (bf16[1536,128]{1,0:T(8,128)(2,1)S(1)}, bf16[1536,128]{1,0:T(8,128)(2,1)S(1)}, u32[]{:S(2)}, u32[]{:S(2)}) collective-permute-start(bf16[1536,128]{1,0:T(8,128)(2,1)S(1)} %collective-permute-done.19.g2), channel_id=1, source_target_pairs={{0,16},{16,0},{1,17},{17,1},{2,18},{18,2},{3,19},{19,3},{4,20},{20... | collective-permute-start | bytes 1179656 | tf_op jit(solution)/shard_map/ppermute | solution.py:25
  42.0 24.3 %collective-permute-start.24 = (bf16[1536,128]{1,0:T(8,128)(2,1)S(1)}, bf16[1536,128]{1,0:T(8,128)(2,1)S(1)}, u32[]{:S(2)}, u32[]{:S(2)}) collective-permute-start(bf16[1536,128]{1,0:T(8,128)(2,1)S(1)} %collective-permute-done.20.g3), channel_id=1, source_target_pairs={{0,16},{16,0},{1,17},{17,1},{2,18},{18,2},{3,19},{19,3},{4,20},{20... | collective-permute-start | bytes 1179656 | tf_op jit(solution)/shard_map/ppermute | solution.py:25
  42.1 2.7 %collective-permute-start.9 = (bf16[1184,128]{1,0:T(8,128)(2,1)S(1)}, bf16[1184,128]{1,0:T(8,128)(2,1)S(1)}, u32[]{:S(2)}, u32[]{:S(2)}) collective-permute-start(bf16[1184,128]{1,0:T(8,128)(2,1)S(1)} %collective-permute-done.6.a3), channel_id=1, source_target_pairs={{0,16},{16,0},{1,17},{17,1},{2,18},{18,2},{3,19},{19,3},{4,20},{20... | collective-permute-start | bytes 909320 | tf_op jit(solution)/shard_map/ppermute | solution.py:25
  46.9 3.8 %collective-permute-start.10 = (f32[2,4,4,128]{3,2,1,0:T(4,128)S(1)}, f32[2,4,4,128]{3,2,1,0:T(4,128)S(1)}, u32[]{:S(2)}, u32[]{:S(2)}) collective-permute-start(f32[2,4,4,128]{3,2,1,0:T(4,128)S(1)} %get-tuple-element.49.total), channel_id=1, source_target_pairs={{0,4},{4,0},{8,12},{12,8},{1,5},{5,1},{9,13},{13,9},{2,6},{6,2},{1... | collective-permute-start | bytes 49160 | tf_op jit(solution)/shard_map/ppermute | solution.py:280
  50.7 5.0 %collective-permute-start.11 = (f32[2,4,4,128]{3,2,1,0:T(4,128)S(1)}, f32[2,4,4,128]{3,2,1,0:T(4,128)S(1)}, u32[]{:S(2)}, u32[]{:S(2)}) collective-permute-start(f32[2,4,4,128]{3,2,1,0:T(4,128)S(1)} %get-tuple-element.50.total), channel_id=1, source_target_pairs={{0,12},{4,8},{8,4},{12,0},{1,13},{5,9},{9,5},{13,1},{2,14},{6,10},... | collective-permute-start | bytes 49160 | tf_op jit(solution)/shard_map/ppermute | solution.py:280
  55.7 1.3 %collective-permute-start.12 = (f32[2,4,4,128]{3,2,1,0:T(4,128)S(1)}, f32[2,4,4,128]{3,2,1,0:T(4,128)S(1)}, u32[]{:S(2)}, u32[]{:S(2)}) collective-permute-start(f32[2,4,4,128]{3,2,1,0:T(4,128)S(1)} %get-tuple-element.52.total), channel_id=1, source_target_pairs={{0,16},{16,0},{1,17},{17,1},{2,18},{18,2},{3,19},{19,3},{4,20},{20... | collective-permute-start | bytes 49160 | tf_op jit(solution)/shard_map/ppermute | solution.py:280
  57.0 3.8 %collective-permute-start.13 = (f32[2,4,4,128]{3,2,1,0:T(4,128)S(1)}, f32[2,4,4,128]{3,2,1,0:T(4,128)S(1)}, u32[]{:S(2)}, u32[]{:S(2)}) collective-permute-start(f32[2,4,4,128]{3,2,1,0:T(4,128)S(1)} %get-tuple-element.54.total), channel_id=1, source_target_pairs={{0,32},{32,0},{64,96},{96,64},{1,33},{33,1},{65,97},{97,65},{2,34}... | collective-permute-start | bytes 49160 | tf_op jit(solution)/shard_map/ppermute | solution.py:280
  60.8 5.5 %collective-permute-start.14 = (f32[2,4,4,128]{3,2,1,0:T(4,128)S(1)}, f32[2,4,4,128]{3,2,1,0:T(4,128)S(1)}, u32[]{:S(2)}, u32[]{:S(2)}) collective-permute-start(f32[2,4,4,128]{3,2,1,0:T(4,128)S(1)} %get-tuple-element.56.total), channel_id=1, source_target_pairs={{0,96},{32,64},{64,32},{96,0},{1,97},{33,65},{65,33},{97,1},{2,98}... | collective-permute-start | bytes 49160 | tf_op jit(solution)/shard_map/ppermute | solution.py:280
  69.8 11.1 %collective-permute-start.25 = (bf16[4,16,2048]{2,1,0:T(8,128)(2,1)S(1)}, bf16[4,16,2048]{2,1,0:T(8,128)(2,1)S(1)}, u32[]{:S(2)}, u32[]{:S(2)}) collective-permute-start(bf16[4,16,2048]{2,1,0:T(8,128)(2,1)S(1)} %get-tuple-element.64), channel_id=1, source_target_pairs={{0,1},{1,2},{2,3},{3,0},{4,5},{5,6},{6,7},{7,4},{8,9},{9,10},{10,1... | collective-permute-start | bytes 786440 | tf_op jit(solution)/shard_map/ppermute | solution.py:25
  74.2 8.9 %collective-permute-start.26 = (bf16[4,16,2048]{2,1,0:T(8,128)(2,1)S(1)}, bf16[4,16,2048]{2,1,0:T(8,128)(2,1)S(1)}, u32[]{:S(2)}, u32[]{:S(2)}) collective-permute-start(bf16[4,16,2048]{2,1,0:T(8,128)(2,1)S(1)} %get-tuple-element.65), channel_id=1, source_target_pairs={{0,3},{1,0},{2,1},{3,2},{4,7},{5,4},{6,5},{7,6},{8,11},{9,8},{10,9... | collective-permute-start | bytes 786440 | tf_op jit(solution)/shard_map/ppermute | solution.py:25
  74.4 11.3 %collective-permute-start.27 = (bf16[4,16,2048]{2,1,0:T(8,128)(2,1)S(1)}, bf16[4,16,2048]{2,1,0:T(8,128)(2,1)S(1)}, u32[]{:S(2)}, u32[]{:S(2)}) collective-permute-start(bf16[4,16,2048]{2,1,0:T(8,128)(2,1)S(1)} %get-tuple-element.66), channel_id=1, source_target_pairs={{0,2},{1,3},{2,0},{3,1},{4,6},{5,7},{6,4},{7,5},{8,10},{9,11},{10,... | collective-permute-start | bytes 786440 | tf_op jit(solution)/shard_map/ppermute | solution.py:25
